TPU v7x, 128 devices: a whole 4x4x4 slice. The times are simulated.
128 devices in a mesh: rep: 2 (over z_hi), fs: 32 (over z_lo, y, x), tp: 2 (over core).
Axes of the slice: x: 4, y: 4, z: 4 (z_hi: 2, z_lo: 2; z = z_hi * 2 + z_lo), core: 2. Of those that a mesh axis runs over, the one named last changes fastest.
Arguments:
- tokens: bfloat16 [65536, 2048], P(('rep', 'fs', 'tp')), may hold values from -6 to 6
- pre_gain: bfloat16 [2048], replicated, may hold values from 0.099609375 to 1.8984375
- gate_weight: bfloat16 [2048, 2816], P('fs', 'tp'), may hold values from -0.125 to 0.125
- value_weight: bfloat16 [2048, 2816], P('fs', 'tp'), may hold values from -0.125 to 0.125
- down_weight: bfloat16 [2816, 2048], P('tp', 'fs'), may hold values from -0.109375 to 0.109375
- post_gain: bfloat16 [2048], replicated, may hold values from 0.099609375 to 1.8984375
Outputs:
- updated: bfloat16 [65536, 2048], P(('rep', 'fs', 'tp'))
All inputs are finite; a program needn't handle non-finite values.
Results may differ from a plain program's by a relative error of at most 0.0055.
Values may be sent and summed in bfloat16 or wider, within the bound.
A program may use at most 128 MiB of HBM per device.

v0:
```python
import jax
import jax.numpy as jnp
from jax import lax
from jax.sharding import Mesh
from jax.sharding import PartitionSpec as P

FS = ("fs_0", "fs_1", "fs_2")
REP_FS_TP = ("rep", "fs_0", "fs_1", "fs_2", "tp")


eps_norm = 1e-06


def in_order(parts, dim):
    lengths = list(parts.shape[1:])
    lengths[dim] *= parts.shape[0]
    return jnp.moveaxis(parts, 0, dim).reshape(lengths)


def sent_to_all(array, axis):
    peers = lax.axis_size(axis)
    return lax.all_to_all(
        jnp.broadcast_to(array[None], (peers, *array.shape)), axis, 0, 0, tiled=True
    )


def gathered_copies(array, axis, dim):
    return in_order(sent_to_all(array, axis), dim)


def in_one_piece(arrays, axis, dim, along):
    both = jnp.concatenate(arrays, axis=along)
    whole, at, finished = (lax.all_gather(both, axis, axis=dim, tiled=True), 0, [])
    for a in arrays:
        finished.append(lax.slice_in_dim(whole, at, at + a.shape[along], axis=along))
        at += a.shape[along]
    return tuple(finished)


def gather_in_order(array, axes, turns):
    parts = array
    for k in turns:
        parts = lax.all_gather(parts, axes[k])
    done = turns[::-1]
    back = [done.index(k) for k in range(len(axes))]
    parts = parts.transpose(*back, *range(len(axes), parts.ndim))
    return parts.reshape(-1, *array.shape)


def gathered_by_axis(array, axes, turns, dim):
    return in_order(gather_in_order(array, axes, turns), dim)


def cut_along(array, dim, peers):
    lengths = array.shape
    parts = array.reshape(*lengths[:dim], peers, lengths[dim] // peers, *lengths[dim + 1 :])
    return jnp.moveaxis(parts, dim, 0)


def sent_and_summed(array, axis, dim):
    parts = cut_along(array, dim, lax.axis_size(axis))
    arrived = lax.all_to_all(parts, axis, split_axis=0, concat_axis=0, tiled=True)
    return arrived.astype(jnp.float32).sum(axis=0)


def rms_rows(values_in, gain):
    floats = values_in.astype(jnp.float32)
    scaled = floats * lax.rsqrt(jnp.mean(floats * floats, -1, keepdims=True) + eps_norm)
    return scaled * gain.astype(jnp.float32)


def shards(tokens, pre_gain, gate_weight, value_weight, down_weight, post_gain):
    normed = rms_rows(tokens, pre_gain).astype(jnp.bfloat16)
    group_rows = gathered_copies(normed, "tp", 0)
    pieces = in_one_piece((gate_weight, value_weight), FS, 0, 1)
    gate_add = jnp.dot(group_rows, pieces[0], preferred_element_type=jnp.float32)
    value_add = jnp.dot(group_rows, pieces[1], preferred_element_type=jnp.float32)
    down_full = gathered_by_axis(down_weight, FS, (0, 1, 2), 1)
    hidden = (jax.nn.silu(gate_add) * value_add).astype(jnp.bfloat16)
    branch = sent_and_summed(
        jnp.dot(hidden, down_full, preferred_element_type=jnp.float32).astype(jnp.bfloat16), "tp", 0
    ).astype(jnp.bfloat16)
    updated = tokens.astype(jnp.float32) + 0.5 * rms_rows(branch, post_gain)
    return updated.astype(jnp.bfloat16)


def solution(mesh):
    torus = Mesh(
        mesh.devices.reshape(mesh.shape["rep"], 2, 4, 4, mesh.shape["tp"]),
        ("rep", "fs_0", "fs_1", "fs_2", "tp"),
    )
    in_specs = (P(REP_FS_TP, None), P(), P(FS, "tp"), P(FS, "tp"), P("tp", FS), P())
    out_specs = P(REP_FS_TP, None)
    return jax.shard_map(
        shards, mesh=torus, in_specs=in_specs, out_specs=out_specs, check_vma=False
    )
```

profile of v0, /device:TPU:1, one launch (start us, length us, event | category | flops | bytes accessed | tf_op | source)
XLA Modules:
  0.0 340.0 jit_solution(4226136508492825143)
XLA Ops:
  6.5 0.0 copy-start
  6.5 0.0 all-gather.9.cloned.1.call-start
  6.5 7.8 %all-gather = bf16[2816,64]{0,1:T(8,128)(2,1)S(1)} all-gather(bf16[1408,64]{0,1:T(8,128)(2,1)} %param.10), channel_id=2, replica_groups=mesh['rep'=2,'fs_0'=2,'fs_1'=4,'fs_2'=4,'tp'=2] {'fs_0'}, dimensions={0}, use_global_device_ids=true | all-gather | bytes 540672 | tf_op jit(solution)/shard_map/all_gather | solution.py:43
  14.3 0.8 copy.14
  15.1 0.0 all-gather.9.cloned.1.call-update
  15.1 0.0 all-gather.11.cloned.1.call-start
  15.1 28.1 %all-gather.9.cloned.1.call-done = bf16[8,1408,64]{1,2,0:T(8,128)(2,1)} async-done(((bf16[2,1408,64]{1,2,0:T(8,128)(2,1)}), bf16[8,1408,64]{1,2,0:T(8,128)(2,1)}) %all-gather.9.cloned.1.call-update) | async-done | bytes 1441808 | tf_op jit(solution)/shard_map/all_gather | solution.py:43
  43.2 0.0 all-gather.11.cloned.1.call-update
  43.2 0.0 all-gather.7.cloned.1.call-start
  43.3 1.8 pad_maximum_fusion
  45.0 0.0 all-gather.7.cloned.1.call-update
  45.1 0.7 convert_element_type.28
  45.8 0.0 copy-done
  45.8 0.5 fusion.12
  46.3 0.6 fusion.14
  46.8 2.6 broadcast_in_dim.2
  49.4 0.0 copy-start.1
  49.4 6.6 %all-to-all-start = ((bf16[2,512,2048]{2,1,0:T(8,128)(2,1)}), bf16[2,512,2048]{2,1,0:T(8,128)(2,1)}, u32[]{:S(2)}, u32[]{:S(2)}) async-start(bf16[2,512,2048]{2,1,0:T(8,128)(2,1)} %broadcast_in_dim.2), calls=%async_computation | async-start | bytes 8388608 | tf_op jit(solution)/shard_map/all_to_all | solution.py:22
  56.0 0.0 copy-done.1
  56.0 50.5 %all-gather.11.cloned.1.call-done = bf16[16,2,1408,64]{2,3,1,0:T(8,128)(2,1)} async-done(((bf16[4,2,1408,64]{2,3,1,0:T(8,128)(2,1)}), bf16[16,2,1408,64]{2,3,1,0:T(8,128)(2,1)}) %all-gather.11.cloned.1.call-update) | async-done | bytes 5767184 | tf_op jit(solution)/shard_map/all_gather | solution.py:43
  106.5 5.7 %copy.11 = bf16[2,4,4,1408,64]{3,4,2,1,0:T(8,128)(2,1)} copy(bf16[2,4,4,1408,64]{3,4,0,1,2:T(8,128)(2,1)} %bitcast.18) | data formatting | bytes 11534336 | tf_op jit(solution)/shard_map/transpose | solution.py:46
  112.2 0.0 all-to-all-done
  112.2 149.4 %all-gather.7.cloned.1.call-done = bf16[2048,2816]{1,0:T(8,128)(2,1)} async-done(((bf16[64,2816]{1,0:T(8,128)(2,1)}), bf16[2048,2816]{1,0:T(8,128)(2,1)}) %all-gather.7.cloned.1.call-update) | async-done | bytes 11534352 | tf_op jit(solution)/shard_map/all_gather | solution.py:33
  261.6 11.7 %fusion.2 = f32[1024,1408]{1,0:T(8,128)} fusion(bf16[1024,2048]{1,0:T(8,128)(2,1)} %bitcast, bf16[2048,2816]{1,0:T(8,128)(2,1)} %all-gather.7.cloned.1.call-done), kind=kOutput, calls=%fused_computation.5 | convolution fusion | flops 5905580032 | bytes 15728640 | tf_op jit(solution)/shard_map/dot_general | solution.py:76
  273.3 20.6 %fusion.16 = bf16[1024,2048]{1,0:T(8,128)(2,1)} fusion(bf16[1408,2048]{0,1:T(8,128)(2,1)} %bitcast.19, f32[1024,1408]{1,0:T(8,128)} %fusion.2, bf16[1024,2048]{1,0:T(8,128)(2,1)} %bitcast, bf16[2048,2816]{1,0:T(8,128)(2,1)} %all-gather.7.cloned.1.call-done), kind=kOutput, calls=%fused_computation.18 | convolution fusion | flops 11821907968 | bytes 25690112 | tf_op jit(solution)/shard_map/dot_general | solution.py:81
  293.9 31.5 %all_to_all.10 = bf16[2,512,2048]{2,1,0:T(8,128)(2,1)} all-to-all(bf16[2,512,2048]{2,1,0:T(8,128)(2,1)} %bitcast.20), channel_id=1, replica_groups=mesh['rep'=2,'fs_0'=2,'fs_1'=4,'fs_2'=4,'tp'=2] {'tp'}, dimensions={0} | all-to-all | bytes 8388608 | tf_op jit(solution)/shard_map/all_to_all | solution.py:62
  325.4 3.4 reduce_sum.31
  328.8 0.5 fusion.9
  329.3 4.2 %fusion.15 = bf16[512,2048]{1,0:T(8,128)(2,1)} fusion(bf16[512,2048]{1,0:T(8,128)(2,1)S(1)} %reduce_sum.31, bf16[512,2048]{1,0:T(8,128)(2,1)} %param.6, f32[2048]{0:T(1024)S(1)} %convert_element_type.33, f32[512]{0:T(512)S(1)} %add_rsqrt_fusion), kind=kLoop, calls=%fused_computation.17 | loop fusion | flops 7340032 | bytes 6301696 | tf_op jit(solution)/shard_map/convert_element_type | solution.py:84
  (3 shorter events, 0.0 us)
Async XLA Ops:
  6.5 39.2 %copy-start = (bf16[512,2048]{1,0:T(8,128)(2,1)S(1)}, bf16[512,2048]{1,0:T(8,128)(2,1)}, u32[]{:S(2)}) copy-start(bf16[512,2048]{1,0:T(8,128)(2,1)} %param.6) | copy-start | bytes 6291460
  6.5 36.7 %all-gather.9.cloned.1.call-start = ((), (), s32[]{:S(2)}) async-start(), calls=%async_computation.3 | async-start | bytes 1802240 | tf_op jit(solution)/shard_map/all_gather | solution.py:43
  15.1 91.4 %all-gather.11.cloned.1.call-start = ((), (), s32[]{:S(2)}) async-start(), calls=%async_computation.4 | async-start | bytes 7208960 | tf_op jit(solution)/shard_map/all_gather | solution.py:43
  43.2 218.4 %all-gather.7.cloned.1.call-start = ((), (), s32[]{:S(2)}) async-start(), calls=%async_computation.2 | async-start | bytes 11894784 | tf_op jit(solution)/shard_map/all_gather | solution.py:33
  49.4 6.6 %copy-start.1 = (bf16[2048]{0:T(1024)(128)(2,1)S(1)}, bf16[2048]{0:T(1024)(128)(2,1)}, u32[]{:S(2)}) copy-start(bf16[2048]{0:T(1024)(128)(2,1)} %param.11) | copy-start | bytes 12292
  49.4 62.7 %all-to-all-start = ((bf16[2,512,2048]{2,1,0:T(8,128)(2,1)}), bf16[2,512,2048]{2,1,0:T(8,128)(2,1)}, u32[]{:S(2)}, u32[]{:S(2)}) async-start(bf16[2,512,2048]{2,1,0:T(8,128)(2,1)} %broadcast_in_dim.2), calls=%async_computation | async-start | bytes 8388608 | tf_op jit(solution)/shard_map/all_to_all | solution.py:22
Sparse Core Ops, SparseCore 0:
  15.2 27.9 all-gather.8
  44.9 61.5 all-gather.10
  108.1 153.3 all-gather.6
where the time goes:
time: 341 us; the launch traced here: 340 us
  waiting for transfers between devices  228 us (67%)
  blocking collectives  39.3 us (12%)
  matrix products  32.3 us (9%)
  between operations  13.1 us (4%)
  other arithmetic  11.6 us (3%)
  local copies, waits for them, and re-layouts  9.03 us (3%)
  starting transfers between devices  6.64 us (2%)
    all_gather x1, waiting for transfers between devices, in_one_piece(): lax.all_gather(both, axis, axis=dim, tiled=True)  149 us
    all_gather x2, waiting for transfers between devices, gather_in_order(): parts = lax.all_gather(parts, axes[k])  78.6 us
    all_to_all x1, blocking collectives, sent_and_summed(): lax.all_to_all(parts, axis, split_axis=0, concat_axis=0, tiled=True)  31.5 us
    dot_general x1, matrix products, shards(): jnp.dot(hidden, down_full, preferred_element_type=jnp.float32)  20.6 us
    dot_general x1, matrix products, shards(): jnp.dot(group_rows, pieces[0], preferred_element_type=jnp.float32)  11.7 us
    all_gather x1, blocking collectives, gather_in_order(): parts = lax.all_gather(parts, axes[k])  7.76 us
  transfers between devices with their start and end apart: 4, of which 3 were waited for; matrix products, arithmetic and copies ran while one was open for 3% of the time, Pallas kernels for 0%

commit v1 on v0

v1 whole, which is shorter than its diff:
```python
import jax
import jax.numpy as jnp
from jax import lax
from jax.experimental import pallas as pl
from jax.experimental.pallas import tpu as pltpu
from jax.sharding import PartitionSpec as P

D, F, Q, TOK = 2048, 1408, 704, 512
SENT = 2048
EPS = 1e-06
F32, BF16 = jnp.float32, jnp.bfloat16


class Copy:
    def __init__(self, src, dst, here, send_sem, recv_sem, to):
        make = pltpu.make_async_remote_copy
        kind = dict(device_id=to, device_id_type=pl.DeviceIdType.MESH)
        self.out = make(src_ref=src, dst_ref=dst, send_sem=send_sem, recv_sem=recv_sem, **kind)
        self.into = make(src_ref=here, dst_ref=here, send_sem=send_sem, recv_sem=recv_sem, **kind)

    def start(self):
        self.out.start()

    def arrived(self):
        self.into.wait_recv()

    def left(self):
        self.out.wait_send()


def ring_copies(block, half, to_a, to_b, send, recv):
    c = []
    for way in (1, -1):
        c.append((block(0, 0), block(-way, 0), to_a[way]))
    for way, h in ((1, 0), (-1, 1)):
        c.append((half(-way, 0, h), half(2, 0, h), to_a[way]))
    for way in (1, -1):
        for oa in (0, -1, 1, 2):
            c.append((block(oa, 0), block(oa, -way), to_b[way]))
    for way, h in ((1, 0), (-1, 1)):
        for oa in (0, -1, 1, 2):
            c.append((half(oa, -way, h), half(oa, 2, h), to_b[way]))
    return [Copy(ref, ref, here, send.at[i], recv.at[i], to) for i, (ref, here, to) in enumerate(c)]


def kernel(tok_in, pre_ref, gate_in, value_in, down_in, post_ref, out_ref, tok, wg, wv, wd, dd, dz, w, d, t, acc, hid, ps,
           pr, rp, zs, zr, own, os_, or_, load, ag_s, ag_r, zw_s, zw_r, tk_s, tk_r, p2_s, p2_r):
    rep, fs, core = lax.axis_index("rep"), lax.axis_index("fs"), lax.axis_index("tp")
    zlo, y, x = fs // 16, (fs // 4) % 4, fs % 4
    z = rep * 2 + zlo

    def device(dz_=0, dy=0, dx=0, other=False):
        zz, yy, xx = (z + dz_ + 4) % 4, (y + dy + 4) % 4, (x + dx + 4) % 4
        return {"rep": zz // 2, "fs": (zz % 2) * 16 + yy * 4 + xx, "tp": 1 - core if other else core}

    to_x = {1: device(dx=1), -1: device(dx=-1)}
    to_y = {1: device(dy=1), -1: device(dy=-1)}
    to_z = {1: device(dz_=1), -1: device(dz_=-1)}
    partner = device(other=True)

    loads = [
        pltpu.make_async_copy(gate_in, wg, load.at[0]),
        pltpu.make_async_copy(value_in, wv, load.at[1]),
        pltpu.make_async_copy(down_in, wd.at[0:64], load.at[2]),
        pltpu.make_async_copy(down_in, wd.at[64:128], load.at[3]),
        pltpu.make_async_copy(tok_in, tok, load.at[4]),
    ]
    for c in loads:
        c.start()

    barrier = pltpu.get_barrier_semaphore()
    for peer in (*to_x.values(), *to_y.values(), *to_z.values(), partner):
        pl.semaphore_signal(barrier, inc=1, device_id=peer, device_id_type=pl.DeviceIdType.MESH)

    lanes = lax.broadcasted_iota(jnp.int32, (64, 128), 1)
    low = lanes < 64
    swap = lambda v: pltpu.roll(v, 64, 1)

    loads[0].wait()
    loads[1].wait()
    place = (y * 4 + x) * 64
    for q in (0, 1):
        at = pl.multiple_of(place + (zlo + q) % 2 * (2048 - place), 64)
        g5, v5 = wg[:, 640:768].astype(F32), wv[:, 640:768].astype(F32)
        first = 768 * q
        w[pl.ds(at, 64), 0:640] = wg[:, first:first + 640]
        w[pl.ds(at, 64), 640:1280] = wv[:, first:first + 640]
        mixed = jnp.where(low, g5, swap(v5)) if q == 0 else jnp.where(low, swap(g5), v5)
        w[pl.ds(at, 64), 1280:1408] = mixed.astype(BF16)

    def slot(oy, ox):
        return (y + oy + 4) % 4, (x + ox + 4) % 4

    def gv(first, rows, h):
        def ref(oa, ob):
            yy, xx = slot(ob, oa) if first == "x" else slot(oa, ob)
            at = (yy * 4 + xx) * 64 if first == "x" else 1024 + (xx * 4 + yy) * 64
            return w.at[pl.ds(pl.multiple_of(at + h * rows, rows), rows)]

        return ref

    def dn(first, rows, h):
        def ref(oa, ob):
            yy, xx = slot(ob, oa) if first == "x" else slot(oa, ob)
            at = (0 if first == "x" else 352) + h * rows
            return d.at[at:at + rows, pl.ds(pl.multiple_of((yy * 4 + xx) * 128, 128), 128)]

        return ref

    items = []
    for i, (make, rows, first) in enumerate(((gv, 64, "x"), (gv, 64, "y"), (dn, 352, "x"), (dn, 352, "y"))):
        halves = [make(first, rows // 2, h) for h in (0, 1)]
        half = lambda oa, ob, h, halves=halves: halves[h](oa, ob)
        a, b = (to_x, to_y) if first == "x" else (to_y, to_x)
        items.append(ring_copies(make(first, rows, 0), half, a, b, ag_s.at[i], ag_r.at[i]))
    A, B, C, E = items

    def send(item, *which):
        for i in which:
            item[i].start()

    def recv(item, *which):
        for i in which:
            item[i].arrived()

    def rows_of(ref, at, n):
        return ref.at[pl.ds(pl.multiple_of(at, n), n)]

    zw = []
    for h, way in ((0, 1), (1, -1)):
        src = w.at[2048 + 32 * h:2080 + 32 * h]
        dst = rows_of(w, 1024 + (x * 4 + y) * 64 + 32 * h, 32)
        zw.append(Copy(src, dst, dst, zw_s.at[h], zw_r.at[h], to_z[way]))
    for h, way in ((0, 1), (1, -1)):
        part = pl.ds(352 * h, 352)
        zw.append(Copy(dd.at[1 - zlo, part], dz.at[part], dz.at[part], zw_s.at[2 + h], zw_r.at[2 + h], to_z[way]))

    pl.semaphore_wait(barrier, 7)
    send(A, 0, 1)
    zw[0].start()
    zw[1].start()
    send(A, 4, 8)

    loads[2].wait()
    loads[3].wait()
    for i in range(11):
        turned = wd[:, i * 128:(i + 1) * 128].astype(F32).T.astype(BF16)
        at = i * 128
        if i < 5:
            dd[0, at:at + 128] = turned
        elif i == 5:
            dd[0, 640:704] = turned[0:64]
            dd[1, 640:704] = turned[64:128]
        else:
            dd[1, at - 768:at - 640] = turned
    zw[2].start()
    zw[3].start()

    def group_rows(at, n):
        return t.at[:, pl.ds(at, n)]

    tok_z, tok_c, tok_f = [], [], []
    for c in range(4):
        r = 128 * c
        here = group_rows(1024 + r, 128)
        tok_z.append(Copy(group_rows(SENT + r, 128), here, here, tk_s.at[c], tk_r.at[c], to_z[1 if c < 2 else -1]))
        here = group_rows(512 + r, 128)
        tok_c.append(Copy(group_rows(r, 128), here, here, tk_s.at[4 + c], tk_r.at[4 + c], partner))
        here = group_rows(1536 + r, 128)
        tok_f.append(Copy(group_rows(1024 + r, 128), here, here, tk_s.at[8 + c], tk_r.at[8 + c], partner))
    loads[4].wait()
    gain = pre_ref[...].astype(F32)
    low32 = lax.broadcasted_iota(jnp.int32, (32, 128), 1) < 64

    def norm(r):
        v = tok[pl.ds(r, 32), :].astype(F32)
        v = v * lax.rsqrt(jnp.mean(v * v, axis=-1, keepdims=True) + EPS) * gain
        for k in (0, 1):
            straight = pl.multiple_of((zlo + k) % 2 * SENT + r, 32)
            turned = pl.multiple_of((zlo + k + 1) % 2 * SENT + r, 32)
            tiles = [v[:, k * 1024 + 128 * i:k * 1024 + 128 * (i + 1)] for i in range(8)]
            flipped = [swap(s) for s in tiles]
            for i in range(8):
                t[i // 2, pl.ds(straight, 32), 128 * (i % 2):128 * (i % 2 + 1)] = tiles[i].astype(BF16)
            for xx in range(4):
                for p in (0, 1):
                    one, two = 4 * p + xx // 2, 4 * p + 2 + xx // 2
                    if xx % 2 == 0:
                        out = jnp.where(low32, tiles[one], flipped[two])
                    else:
                        out = jnp.where(low32, flipped[one], tiles[two])
                    t[4 + xx, pl.ds(turned, 32), 128 * p:128 * (p + 1)] = out.astype(BF16)

    for c in (0, 2, 1, 3):
        pl.loop(0, 4)(lambda i, c=c: norm(pl.multiple_of(c * 128 + i * 32, 32)))
        tok_z[c].start()
        tok_c[c].start()
        if c == 2:
            zw[0].arrived()
            zw[1].arrived()
            send(B, 0, 1, 4, 8)
            recv(A, 0, 1)
            send(A, 2, 3, 5, 9)

    def gates(groups, row, count, first):
        def step(i):
            r = pl.multiple_of(row + i * 512, 512)
            for n in range(0, F, 256):
                m = min(256, F - n)
                total = None if first else acc[pl.ds(r, 512), n:n + m]
                for g in groups:
                    part = jnp.dot(t[g, pl.ds(r, 512), :], w[pl.ds(pl.multiple_of(g * 256, 256), 256), n:n + m],
                                   preferred_element_type=F32)
                    total = part if total is None else total + part
                acc[pl.ds(r, 512), n:n + m] = total

        pl.loop(0, count // 512)(step)

    recv(B, 0, 1)
    send(B, 2, 3, 5, 9)
    send(A, 6, 10)
    send(B, 6, 10)
    recv(A, 4, 8)
    send(A, 12, 16)
    recv(B, 4, 8)
    send(B, 12, 16)

    zw[2].arrived()
    zw[3].arrived()
    tile0 = pl.multiple_of((y * 4 + x) * 128, 128)
    own_half = (lax.broadcasted_iota(jnp.int32, (Q, 128), 1) < 64) == (zlo == 0)
    d[0:Q, pl.ds(tile0, 128)] = jnp.where(own_half, dd[zlo].astype(F32), dz[...].astype(F32)).astype(BF16)
    d[Q:768, :] = jnp.zeros((64, D), BF16)

    for c in range(4):
        tok_c[c].arrived()
    recv(A, 2, 3)
    send(A, 7, 11)
    recv(B, 2, 3)
    send(B, 7, 11)
    for c in (0, 2):
        tok_z[c].arrived()
        tok_f[c].start()
    gates((y, 4 + x), 0, 1024, True)
    recv(A, 5, 9)
    send(A, 13, 17)
    recv(B, 5, 9)
    send(B, 13, 17)
    recv(A, 6, 10)
    send(A, 14, 18)
    recv(B, 6, 10)
    send(B, 14, 18)
    for c in (1, 3):
        tok_z[c].arrived()
        tok_f[c].start()
    recv(A, 7, 11)
    send(A, 15, 19)
    recv(B, 7, 11)
    send(B, 15, 19)
    send(C, 0, 1)
    send(E, 0, 1)
    send(C, 4, 8)
    send(E, 4, 8)
    for c in range(4):
        tok_f[c].arrived()
    gates((y, 4 + x), 1024, 1024, True)
    up, dn_, rt, lf = (y + 1) % 4, (y + 3) % 4, (x + 1) % 4, (x + 3) % 4
    near = (up, dn_, 4 + rt, 4 + lf)
    gates(near, 1024, 1024, False)
    recv(A, 12, 16, 13, 17, 14, 18, 15, 19)
    recv(B, 12, 16, 13, 17, 14, 18, 15, 19)
    far = ((y + 2) % 4, 4 + (x + 2) % 4)
    gates(far, 1024, 1024, False)

    low128 = lax.broadcasted_iota(jnp.int32, (128, 128), 1) < 64

    def hide(row, count):
        def step(i):
            r = pl.multiple_of(row + i * 128, 128)
            for n in range(0, 640, 128):
                g = acc[pl.ds(r, 128), n:n + 128]
                h = g / (1 + jnp.exp(-g)) * acc[pl.ds(r, 128), 640 + n:768 + n]
                hid[pl.ds(r, 128), n:n + 128] = h.astype(BF16)
            m = acc[pl.ds(r, 128), 1280:1408]
            h = m / (1 + jnp.exp(-m)) * swap(m)
            hid[pl.ds(r, 128), 640:768] = jnp.where(low128, h, 0).astype(BF16)

        pl.loop(0, count // 128)(step)

    hide(1024, 1024)

    def tile_of(oy, ox):
        yy, xx = slot(oy, ox)
        return yy * 4 + xx

    back = []
    tiles = [(0, 0), (0, 1), (0, -1), (1, 0), (-1, 0), (1, 1), (1, -1), (-1, 1), (-1, -1), (0, 2), (2, 0), (2, 1), (2, -1),
             (1, 2), (-1, 2), (2, 2)]

    def remote(k):
        j = tile_of(*tiles[k])
        cols = pl.ds(pl.multiple_of(j * 128, 128), 128)

        def part(row):
            return jnp.dot(hid[row:row + 512, :], d[:, cols], preferred_element_type=F32).astype(BF16)

        ps[j] = part(1536)
        over = Copy(ps.at[j], pr.at[j], pr.at[j], p2_s.at[3 * k], p2_r.at[3 * k], partner)
        over.start()
        rp[j] = part(1024)
        home = [Copy(zs.at[j, h], zr.at[j, h], zr.at[j, h], p2_s.at[3 * k + 1 + h], p2_r.at[3 * k + 1 + h], to_z[way])
                for h, way in ((0, -1), (1, 1))]
        back.append((j, over, home))

    def pass_on(k):
        j, over, home = back[k]
        over.arrived()
        both = (rp[j].astype(F32) + pr[j].astype(F32)).astype(BF16)
        zs[j, 0] = both[0:256]
        zs[j, 1] = both[256:512]
        home[0].start()
        home[1].start()

    def run(ks):
        for k in ks:
            remote(k)
            if k > 0:
                pass_on(k - 1)

    run([0])
    recv(C, 0, 1)
    send(C, 2, 3, 5, 9)
    recv(E, 0, 1)
    send(E, 2, 3, 5, 9)
    send(C, 6, 10)
    send(E, 6, 10)
    recv(C, 4, 8)
    send(C, 12, 16)
    recv(E, 4, 8)
    send(E, 12, 16)
    run([1, 2, 3, 4])
    recv(C, 2, 3)
    send(C, 7, 11)
    recv(E, 2, 3)
    send(E, 7, 11)
    recv(C, 5, 9)
    send(C, 13, 17)
    recv(E, 5, 9)
    send(E, 13, 17)
    recv(C, 6, 10)
    send(C, 14, 18)
    recv(E, 6, 10)
    send(E, 14, 18)
    run([5, 6, 7, 8])
    recv(C, 7, 11)
    send(C, 15, 19)
    recv(E, 7, 11)
    send(E, 15, 19)
    recv(C, 12, 16)
    recv(E, 12, 16)
    run([9, 10])
    recv(C, 13, 14, 15, 17, 18, 19)
    recv(E, 13, 14, 15, 17, 18, 19)
    run([11, 12, 13, 14, 15])
    pass_on(15)

    gates(near + far, 0, 1024, False)
    hide(0, 1024)
    across = []
    for n in range(8):
        cols = slice(256 * n, 256 * (n + 1))
        os_[:, cols] = jnp.dot(hid[512:1024, :], d[:, cols], preferred_element_type=F32).astype(BF16)
        across.append(Copy(os_.at[:, cols], or_.at[:, cols], or_.at[:, cols], p2_s.at[48 + n], p2_r.at[48 + n], partner))
        across[n].start()
        own[:, cols] = jnp.dot(hid[0:512, :], d[:, cols], preferred_element_type=F32).astype(BF16)
    for c in across:
        c.arrived()
    for _, _, home in back:
        home[0].arrived()
        home[1].arrived()

    post = post_ref[...].astype(F32)
    low16 = lax.broadcasted_iota(jnp.int32, (16, 128), 1) < 64

    def finish(h, i):
        r = pl.multiple_of(i * 16, 16)
        row = pl.multiple_of(h * 256 + r, 16)
        b, square = [], jnp.zeros((16, 128), F32)
        for j in range(16):
            cols = slice(128 * j, 128 * (j + 1))
            v = own[pl.ds(row, 16), cols].astype(F32) + or_[pl.ds(row, 16), cols].astype(F32)
            v = (v + zr[j, h, pl.ds(r, 16), :].astype(F32)).astype(BF16).astype(F32)
            square += v * v
            b.append(v)
        scale = 0.5 * lax.rsqrt(jnp.sum(square, axis=-1, keepdims=True) * (1 / D) + EPS)
        for j in range(16):
            one, two = b[2 * (j % 8)], b[2 * (j % 8) + 1]
            v = jnp.where(low16, one, swap(two)) if j < 8 else jnp.where(low16, swap(one), two)
            cols = slice(128 * j, 128 * (j + 1))
            v = tok[pl.ds(row, 16), cols].astype(F32) + v * scale * post[:, cols]
            tok[pl.ds(row, 16), cols] = v.astype(BF16)

    stores = []
    for h in (0, 1):
        pl.loop(0, 16)(lambda i, h=h: finish(h, i))
        rows = pl.ds(256 * h, 256)
        stores.append(pltpu.make_async_copy(tok.at[rows], out_ref.at[rows], load.at[5 + h]))
        stores[h].start()

    for c in A + B + C + E + zw + tok_z + tok_c + tok_f + across:
        c.left()
    for _, over, home in back:
        over.left()
        home[0].left()
        home[1].left()
    for c in stores:
        c.wait()


def shards(tokens, pre_gain, gate_weight, value_weight, down_weight, post_gain):
    any_, vmem = pl.BlockSpec(memory_space=pl.ANY), pl.BlockSpec(memory_space=pltpu.VMEM)
    sem = pltpu.SemaphoreType.DMA
    buf = lambda *s, t=BF16: pltpu.VMEM(s, t)
    return pl.pallas_call(
        kernel,
        out_shape=jax.ShapeDtypeStruct((TOK, D), BF16),
        in_specs=[any_, vmem, any_, any_, any_, vmem],
        out_specs=any_,
        scratch_shapes=[
            buf(TOK, D), buf(64, F), buf(64, F), buf(128, F), buf(2, Q, 128), buf(Q, 128), buf(2112, F), buf(768, D),
            buf(8, 2560, 256), buf(2048, F, t=F32), buf(2048, 768), buf(16, 512, 128), buf(16, 512, 128), buf(16, 512, 128),
            buf(16, 2, 256, 128), buf(16, 2, 256, 128), buf(TOK, D), buf(TOK, D), buf(TOK, D),
            sem((7,)), sem((4, 20)), sem((4, 20)), sem((4,)), sem((4,)), sem((12,)), sem((12,)), sem((56,)), sem((56,)),
        ],
        compiler_params=pltpu.CompilerParams(collective_id=0, has_side_effects=True, vmem_limit_bytes=63 * 1024 * 1024),
    )(tokens, pre_gain[None], gate_weight, value_weight, down_weight.T, post_gain[None])


def solution(mesh):
    rows = P(("rep", "fs", "tp"), None)
    in_specs = (rows, P(), P("fs", "tp"), P("fs", "tp"), P("tp", "fs"), P())
    return jax.shard_map(shards, mesh=mesh, in_specs=in_specs, out_specs=rows, check_vma=False)
```

time: 341 us -> 97.4 us (0.29)
  waiting for transfers between devices: 228 us -> 0 us
  Pallas kernels: 0 us -> 91.4 us
  blocking collectives: 39.3 us -> 0 us
  matrix products: 32.3 us -> 0 us
  between operations: 13.1 us -> 0.01 us
  other arithmetic: 11.6 us -> 0 us
  starting transfers between devices: 6.64 us -> 0 us
    all_gather x3 -> x0, waiting for transfers between devices: 228 us -> none  [the longest x1 149 us: in_one_piece(): lax.all_gather(both, axis, axis=dim, tiled=True)]
    pallas_call x0 -> x1, Pallas kernels: none -> 91.4 us  [shards(): pl.pallas_call(kernel, out_shape=jax.ShapeDtypeStruct((TOK, D), BF16), in...]
    dot_general x2 -> x0, matrix products: 32.3 us -> none  [the longest x1 20.6 us: shards(): jnp.dot(hidden, down_full, preferred_element_type=jnp.float32)]
    all_to_all x1 -> x0, blocking collectives: 31.5 us -> none  [sent_and_summed(): lax.all_to_all(parts, axis, split_axis=0, concat_axis=0, tiled=True)]
    all_gather x1 -> x0, blocking collectives: 7.76 us -> none  [gather_in_order(): parts = lax.all_gather(parts, axes[k])]
    all_to_all x1 -> x0, starting transfers between devices: 6.56 us -> none  [sent_to_all(): lax.all_to_all(jnp.broadcast_to(array[None], (peers, *array.shape)), axis...]
    transpose x1 -> x0, local copies, waits for them, and re-layouts: 5.66 us -> none  [gather_in_order(): parts = parts.transpose(*back, *range(len(axes), parts.ndim))]
    convert_element_type x4 -> x0, other arithmetic: 5.42 us -> none  [the longest x1 4.17 us: shards(): return updated.astype(jnp.bfloat16)]
  transfers between devices with their start and end apart: 4 -> 0, of which waited for: 3 -> 0; matrix products, arithmetic and copies ran while one was open for 3% -> 0% of each run, Pallas kernels for 0% -> 0%
where the time goes in v1:
time: 97.4 us; the launch traced here: 97.2 us
  Pallas kernels  91.4 us (94%)
  local copies, waits for them, and re-layouts  5.74 us (6%)
    pallas_call x1, Pallas kernels, shards(): pl.pallas_call(kernel, out_shape=jax.ShapeDtypeStruct((TOK, D), BF16), in...  91.4 us
    unnamed x1, local copies, waits for them, and re-layouts  3.16 us

profile of v1, /device:TPU:1, one launch (start us, length us, event | category | flops | bytes accessed | tf_op | source)
XLA Modules:
  0.0 97.2 jit_solution(6077699443095380382)
XLA Ops:
  0.0 1.3 %broadcast_in_dim.6.pre_ref = bf16[1,2048]{1,0:T(2,128)(2,1)} reshape(bf16[2048]{0:T(1024)(128)(2,1)} %param.7) | data formatting | bytes 8192 | tf_op jit(solution)/shard_map/broadcast_in_dim | solution.py:436
  1.3 1.3 %broadcast_in_dim.7.post_ref = bf16[1,2048]{1,0:T(2,128)(2,1)} reshape(bf16[2048]{0:T(1024)(128)(2,1)} %param.11) | data formatting | bytes 8192 | tf_op jit(solution)/shard_map/broadcast_in_dim | solution.py:436
  2.6 91.4 %shard_map.64 = bf16[512,2048]{1,0:T(8,128)(2,1)} custom-call(bf16[512,2048]{1,0:T(8,128)(2,1)} %tok_in.1, bf16[1,2048]{1,0:T(2,128)(2,1)} %broadcast_in_dim.6.pre_ref, bf16[64,1408]{1,0:T(8,128)(2,1)} %gate_in.1, bf16[64,1408]{1,0:T(8,128)(2,1)} %value_in.1, bf16[64,1408]{1,0:T(8,128)(2,1)} %bitcast.1, bf16[1,2048]{1,0:T(2,128)(2,1)} %broadcast_in_dim.7.post_ref), custom_call_target="tpu_custom_call" | custom-call | tf_op jit(solution)/shard_map/pallas_call | solution.py:424
  94.0 3.2 %copy.8 = bf16[512,2048]{1,0:T(8,128)(2,1)} copy(bf16[512,2048]{1,0:T(8,128)(2,1)} %shard_map.64) | data formatting | bytes 4194304

commit v2 on v1

v2 whole, which is shorter than its diff:
```python
import jax
import jax.numpy as jnp
from jax import lax
from jax.experimental import pallas as pl
from jax.experimental.pallas import tpu as pltpu
from jax.sharding import PartitionSpec as P

D, F, Q, TOK = 2048, 1408, 704, 512
SENT = 2048
EPS = 1e-06
F32, BF16 = jnp.float32, jnp.bfloat16


class Copy:
    def __init__(self, src, dst, here, send_sem, recv_sem, to):
        make = pltpu.make_async_remote_copy
        kind = dict(device_id=to, device_id_type=pl.DeviceIdType.MESH)
        self.out = make(src_ref=src, dst_ref=dst, send_sem=send_sem, recv_sem=recv_sem, **kind)
        self.into = make(src_ref=here, dst_ref=here, send_sem=send_sem, recv_sem=recv_sem, **kind)

    def start(self):
        self.out.start()

    def arrived(self):
        self.into.wait_recv()

    def left(self):
        self.out.wait_send()


def ring_copies(block, half, to_a, to_b, send, recv):
    c = []
    for way in (1, -1):
        c.append((block(0, 0, 0, 0), block(0, 0, way, 0), block(-way, 0, 0, 0), to_a[way]))
    for way, h in ((1, 0), (-1, 1)):
        c.append((half(-way, 0, 0, 0, h), half(-way, 0, way, 0, h), half(2, 0, 0, 0, h), to_a[way]))
    for way in (1, -1):
        for oa in (0, -1, 1, 2):
            c.append((block(oa, 0, 0, 0), block(oa, 0, 0, way), block(oa, -way, 0, 0), to_b[way]))
    for way, h in ((1, 0), (-1, 1)):
        for oa in (0, -1, 1, 2):
            c.append((half(oa, -way, 0, 0, h), half(oa, -way, 0, way, h), half(oa, 2, 0, 0, h), to_b[way]))
    return [Copy(src, dst, here, send.at[i], recv.at[i], to) for i, (src, dst, here, to) in enumerate(c)]


def position(offset):
    return (0, 1, 3, 2)[offset % 4]


def kernel(tok_in, pre_ref, gate_in, value_in, down_in, post_ref, out_ref, tok, wg, wv, wd, dd, dz, w, d, t, acc, hid, ps,
           pr, rp, zs, zr, own, os_, or_, load, ag_s, ag_r, zw_s, zw_r, tk_s, tk_r, p2_s, p2_r):
    rep, fs, core = lax.axis_index("rep"), lax.axis_index("fs"), lax.axis_index("tp")
    zlo, y, x = fs // 16, (fs // 4) % 4, fs % 4
    z = rep * 2 + zlo

    def device(dz_=0, dy=0, dx=0, other=False):
        zz, yy, xx = (z + dz_ + 4) % 4, (y + dy + 4) % 4, (x + dx + 4) % 4
        return {"rep": zz // 2, "fs": (zz % 2) * 16 + yy * 4 + xx, "tp": 1 - core if other else core}

    to_x = {1: device(dx=1), -1: device(dx=-1)}
    to_y = {1: device(dy=1), -1: device(dy=-1)}
    to_z = {1: device(dz_=1), -1: device(dz_=-1)}
    partner = device(other=True)

    loads = [
        pltpu.make_async_copy(gate_in, wg, load.at[0]),
        pltpu.make_async_copy(value_in, wv, load.at[1]),
        pltpu.make_async_copy(down_in, wd.at[0:64], load.at[2]),
        pltpu.make_async_copy(down_in, wd.at[64:128], load.at[3]),
    ] + [pltpu.make_async_copy(tok_in.at[128 * c:128 * c + 128], tok.at[128 * c:128 * c + 128], load.at[4 + c]) for c in range(4)]
    for c in loads:
        c.start()

    barrier = pltpu.get_barrier_semaphore()
    for peer in (*to_x.values(), *to_y.values(), *to_z.values(), partner):
        pl.semaphore_signal(barrier, inc=1, device_id=peer, device_id_type=pl.DeviceIdType.MESH)

    lanes = lax.broadcasted_iota(jnp.int32, (64, 128), 1)
    low = lanes < 64
    swap = lambda v: pltpu.roll(v, 64, 1)

    loads[0].wait()
    loads[1].wait()
    place = (y * 4 + x) * 64
    for q in (0, 1):
        at = pl.multiple_of(place + (zlo + q) % 2 * (2048 - place), 64)
        g5, v5 = wg[:, 640:768].astype(F32), wv[:, 640:768].astype(F32)
        first = 768 * q
        w[pl.ds(at, 64), 0:640] = wg[:, first:first + 640]
        w[pl.ds(at, 64), 640:1280] = wv[:, first:first + 640]
        mixed = jnp.where(low, g5, swap(v5)) if q == 0 else jnp.where(low, swap(g5), v5)
        w[pl.ds(at, 64), 1280:1408] = mixed.astype(BF16)

    def slot(oy, ox):
        return (y + oy + 4) % 4, (x + ox + 4) % 4

    def gv(first, rows, h):
        def ref(oa, ob, ma, mb):
            yy, xx = slot(ob, oa) if first == "x" else slot(oa, ob)
            at = (yy * 4 + xx) * 64 if first == "x" else 1024 + (xx * 4 + yy) * 64
            return w.at[pl.ds(pl.multiple_of(at + h * rows, rows), rows)]

        return ref

    def dn(first, rows, h):
        def ref(oa, ob, ma, mb):
            oa, ob = position(oa - ma), position(ob - mb)
            at = (0 if first == "x" else 352) + h * rows
            n = (ob * 4 + oa if first == "x" else oa * 4 + ob) * 128
            return d.at[at:at + rows, n:n + 128]

        return ref

    items = []
    for i, (make, rows, first) in enumerate(((gv, 64, "x"), (gv, 64, "y"), (dn, 352, "x"), (dn, 352, "y"))):
        halves = [make(first, rows // 2, h) for h in (0, 1)]
        half = lambda oa, ob, ma, mb, h, halves=halves: halves[h](oa, ob, ma, mb)
        a, b = (to_x, to_y) if first == "x" else (to_y, to_x)
        items.append(ring_copies(make(first, rows, 0), half, a, b, ag_s.at[i], ag_r.at[i]))
    A, B, C, E = items

    def send(item, *which):
        for i in which:
            item[i].start()

    def recv(item, *which):
        for i in which:
            item[i].arrived()

    def rows_of(ref, at, n):
        return ref.at[pl.ds(pl.multiple_of(at, n), n)]

    zw = []
    for h, way in ((0, 1), (1, -1)):
        src = w.at[2048 + 32 * h:2080 + 32 * h]
        dst = rows_of(w, 1024 + (x * 4 + y) * 64 + 32 * h, 32)
        zw.append(Copy(src, dst, dst, zw_s.at[h], zw_r.at[h], to_z[way]))
    for h, way in ((0, 1), (1, -1)):
        part = pl.ds(352 * h, 352)
        zw.append(Copy(dd.at[1 - zlo, part], dz.at[part], dz.at[part], zw_s.at[2 + h], zw_r.at[2 + h], to_z[way]))

    def group_rows(at):
        return t.at[:, pl.ds(at, 128)]

    tok_z, tok_c, tok_f = [], [], []
    for c in range(4):
        r = 128 * c
        mine = 1024 + 512 * (c % 2) + 128 * (c // 2)
        here = group_rows(mine)
        tok_z.append(Copy(group_rows(SENT + r), here, here, tk_s.at[c], tk_r.at[c], to_z[1 if c < 2 else -1]))
        here = group_rows(512 + r)
        tok_c.append(Copy(group_rows(r), here, here, tk_s.at[4 + c], tk_r.at[4 + c], partner))
        here = group_rows(mine + 256)
        tok_f.append(Copy(group_rows(mine), here, here, tk_s.at[8 + c], tk_r.at[8 + c], partner))
    gain = pre_ref[...].astype(F32).reshape(1, D)
    low32 = lax.broadcasted_iota(jnp.int32, (32, 128), 1) < 64

    def norm_rows(r):
        v = tok[pl.ds(r, 32), :].astype(F32)
        v = v * lax.rsqrt(jnp.mean(v * v, axis=-1, keepdims=True) + EPS) * gain
        for k in (0, 1):
            straight = pl.multiple_of((zlo + k) % 2 * SENT + r, 32)
            turned = pl.multiple_of((zlo + k + 1) % 2 * SENT + r, 32)
            tiles = [v[:, k * 1024 + 128 * i:k * 1024 + 128 * (i + 1)] for i in range(8)]
            flipped = [swap(s) for s in tiles]
            for i in range(8):
                t[i // 2, pl.ds(straight, 32), 128 * (i % 2):128 * (i % 2 + 1)] = tiles[i].astype(BF16)
            for xx in range(4):
                for p in (0, 1):
                    one, two = 4 * p + xx // 2, 4 * p + 2 + xx // 2
                    if xx % 2 == 0:
                        out = jnp.where(low32, tiles[one], flipped[two])
                    else:
                        out = jnp.where(low32, flipped[one], tiles[two])
                    t[4 + xx, pl.ds(turned, 32), 128 * p:128 * (p + 1)] = out.astype(BF16)

    def norm(c):
        loads[4 + c].wait()
        pl.loop(0, 4)(lambda i: norm_rows(pl.multiple_of(c * 128 + i * 32, 32)))

    def gates(groups, row, count, first):
        def step(i):
            r = pl.multiple_of(row + i * 512, 512)
            for n in range(0, F, 256):
                m = min(256, F - n)
                total = None if first else acc[pl.ds(r, 512), n:n + m]
                for g in groups:
                    part = jnp.dot(t[g, pl.ds(r, 512), :], w[pl.ds(pl.multiple_of(g * 256, 256), 256), n:n + m],
                                   preferred_element_type=F32)
                    total = part if total is None else total + part
                acc[pl.ds(r, 512), n:n + m] = total

        pl.loop(0, count // 512)(step)

    low128 = lax.broadcasted_iota(jnp.int32, (128, 128), 1) < 64

    def hide(row, count):
        def step(i):
            r = pl.multiple_of(row + i * 128, 128)
            for n in range(0, 640, 128):
                g = acc[pl.ds(r, 128), n:n + 128]
                h = g / (1 + jnp.exp(-g)) * acc[pl.ds(r, 128), 640 + n:768 + n]
                hid[pl.ds(r, 128), n:n + 128] = h.astype(BF16)
            m = acc[pl.ds(r, 128), 1280:1408]
            h = m / (1 + jnp.exp(-m)) * swap(m)
            hid[pl.ds(r, 128), 640:768] = jnp.where(low128, h, 0).astype(BF16)

        pl.loop(0, count // 128)(step)

    pending, back = [], []

    def remote(s, rows, cols):
        ys, xs = range(4)[rows], range(4)[cols]
        slots = [(py, px) for py in ys for px in xs]
        for i in range(0, len(slots), 2):
            pair = slots[i:i + 2]
            right = [d[:, (py * 4 + px) * 128:(py * 4 + px + 1) * 128] for py, px in pair]
            right = jnp.concatenate(right, axis=1) if len(pair) == 2 else right[0]
            part = jnp.dot(hid[1024 + 512 * s:1536 + 512 * s, :], right, preferred_element_type=F32).astype(BF16)
            for n, (py, px) in enumerate(pair):
                ps[s, py, px] = part[256:512, 128 * n:128 * (n + 1)]
                rp[s, py, px] = part[0:256, 128 * n:128 * (n + 1)]
        k = 3 * len(back)
        here = pr.at[s, rows, cols]
        over = Copy(ps.at[s, rows, cols], here, here, p2_s.at[k], p2_r.at[k], partner)
        over.start()
        home = []
        for h, way in ((0, -1), (1, 1)):
            here = zr.at[s, h, rows, cols]
            home.append(Copy(zs.at[s, h, rows, cols], here, here, p2_s.at[k + 1 + h], p2_r.at[k + 1 + h], to_z[way]))
        back.append((s, over, home))
        pending.append((s, slots, over, home))
        if len(pending) > 1:
            pass_on()

    def pass_on():
        s, slots, over, home = pending.pop(0)
        over.arrived()
        for py, px in slots:
            both = (rp[s, py, px].astype(F32) + pr[s, py, px].astype(F32)).astype(BF16)
            zs[s, 0, py, px] = both[0:128]
            zs[s, 1, py, px] = both[128:256]
        home[0].start()
        home[1].start()

    norm(0)
    pl.semaphore_wait(barrier, 7)
    zw[0].start()
    zw[1].start()
    send(A, 0, 1, 4, 8)
    tok_z[0].start()
    tok_c[0].start()
    for c in (2, 1, 3):
        norm(c)
        tok_z[c].start()
        tok_c[c].start()

    loads[2].wait()
    loads[3].wait()
    for i in range(11):
        turned = wd[:, i * 128:(i + 1) * 128].astype(F32).T.astype(BF16)
        at = i * 128
        if i < 5:
            dd[0, at:at + 128] = turned
        elif i == 5:
            dd[0, 640:704] = turned[0:64]
            dd[1, 640:704] = turned[64:128]
        else:
            dd[1, at - 768:at - 640] = turned
    zw[2].start()
    zw[3].start()
    d[Q:768, :] = jnp.zeros((64, D), BF16)

    zw[0].arrived()
    zw[1].arrived()
    send(B, 0, 1, 4, 8)
    recv(A, 0, 1)
    send(A, 2, 3, 5, 9)
    recv(B, 0, 1)
    send(B, 2, 3, 5, 9)
    recv(A, 4, 8)
    send(A, 6, 10, 12, 16)
    recv(B, 4, 8)
    send(B, 6, 10, 12, 16)
    for c in range(4):
        tok_c[c].arrived()
    recv(A, 2, 3)
    send(A, 7, 11)
    recv(A, 5, 9)
    send(A, 13, 17)
    recv(B, 2, 3)
    send(B, 7, 11)
    recv(B, 5, 9)
    send(B, 13, 17)
    here, near, far = (y, 4 + x), ((y + 1) % 4, (y + 3) % 4, 4 + (x + 1) % 4, 4 + (x + 3) % 4), ((y + 2) % 4, 4 + (x + 2) % 4)
    gates(here, 0, 512, True)
    tok_z[0].arrived()
    tok_f[0].start()
    tok_z[2].arrived()
    tok_f[2].start()
    recv(A, 6, 10)
    send(A, 14, 18)
    recv(B, 6, 10)
    send(B, 14, 18)
    gates(here, 512, 512, True)
    tok_f[0].arrived()
    tok_f[2].arrived()
    gates(here, 1024, 512, True)
    recv(A, 7, 11)
    send(A, 15, 19)
    recv(B, 7, 11)
    send(B, 15, 19)
    gates(near, 1024, 512, False)
    tok_z[1].arrived()
    tok_f[1].start()
    tok_z[3].arrived()
    tok_f[3].start()

    zw[2].arrived()
    zw[3].arrived()
    own_half = (lax.broadcasted_iota(jnp.int32, (Q, 128), 1) < 64) == (zlo == 0)
    d[0:Q, 0:128] = jnp.where(own_half, dd[zlo].astype(F32), dz[...].astype(F32)).astype(BF16)
    send(C, 0, 1)
    send(E, 0, 1)
    send(C, 4, 8)
    send(E, 4, 8)
    tok_f[1].arrived()
    tok_f[3].arrived()
    gates(here + near, 1536, 512, True)
    recv(A, 12, 16, 13, 17, 14, 18, 15, 19)
    recv(B, 12, 16, 13, 17, 14, 18, 15, 19)
    one, two, last = slice(0, 1), slice(1, 3), slice(3, 4)
    gates(far, 1024, 512, False)
    hide(1024, 512)
    remote(0, one, one)
    gates(far, 1536, 512, False)
    hide(1536, 512)
    remote(1, one, one)
    recv(C, 0, 1)
    send(C, 2, 3, 5, 9)
    recv(E, 0, 1)
    send(E, 2, 3, 5, 9)
    recv(C, 4, 8)
    send(C, 6, 10, 12, 16)
    recv(E, 4, 8)
    send(E, 6, 10, 12, 16)
    for s in (0, 1):
        remote(s, one, two)
        remote(s, two, one)
    recv(C, 2, 3)
    send(C, 7, 11)
    recv(E, 2, 3)
    send(E, 7, 11)
    recv(C, 5, 9)
    send(C, 13, 17)
    recv(E, 5, 9)
    send(E, 13, 17)
    pass_on()
    gates(near, 0, 512, False)
    recv(C, 6, 10)
    send(C, 14, 18)
    recv(E, 6, 10)
    send(E, 14, 18)
    for s in (0, 1):
        remote(s, two, two)
    pass_on()
    recv(C, 7, 11)
    send(C, 15, 19)
    recv(E, 7, 11)
    send(E, 15, 19)
    gates(near, 512, 512, False)
    recv(C, 12, 16)
    recv(E, 12, 16)
    remote(0, one, last)
    remote(0, last, one)
    pass_on()
    gates(far, 0, 1024, False)
    recv(C, 13, 14, 15, 17, 18, 19)
    recv(E, 13, 14, 15, 17, 18, 19)
    remote(0, two, last)
    remote(0, last, two)
    remote(0, last, last)
    remote(1, one, last)
    remote(1, last, one)
    remote(1, two, last)
    remote(1, last, two)
    remote(1, last, last)
    pass_on()

    hide(0, 1024)
    across = []
    for n in range(8):
        cols = slice(256 * n, 256 * (n + 1))
        os_[:, cols] = jnp.dot(hid[512:1024, :], d[:, cols], preferred_element_type=F32).astype(BF16)
        across.append(Copy(os_.at[:, cols], or_.at[:, cols], or_.at[:, cols], p2_s.at[54 + n], p2_r.at[54 + n], partner))
        across[n].start()
        own[:, cols] = jnp.dot(hid[0:512, :], d[:, cols], preferred_element_type=F32).astype(BF16)
    for c in across:
        c.arrived()

    post = post_ref[...].astype(F32).reshape(1, D)
    low16 = lax.broadcasted_iota(jnp.int32, (16, 128), 1) < 64

    def spot(theirs, me):
        o = (theirs - me + 4) % 4
        return o + o // 2 - o // 3 * 2

    spots = [(spot(j // 4, y), spot(j % 4, x)) for j in range(16)]

    def finish(s, h, i):
        r = pl.multiple_of(i * 16, 16)
        row = pl.multiple_of((2 * h + s) * 128 + r, 16)
        b, square = [], jnp.zeros((16, 128), F32)
        for py, px in spots:
            cols = pl.ds(pl.multiple_of((py * 4 + px) * 128, 128), 128)
            v = own[pl.ds(row, 16), cols].astype(F32) + or_[pl.ds(row, 16), cols].astype(F32)
            v = (v + zr[s, h, py, px, pl.ds(r, 16), :].astype(F32)).astype(BF16).astype(F32)
            square += v * v
            b.append(v)
        scale = 0.5 * lax.rsqrt(jnp.sum(square, axis=-1, keepdims=True) * (1 / D) + EPS)
        for j in range(16):
            one, two = b[2 * (j % 8)], b[2 * (j % 8) + 1]
            v = jnp.where(low16, one, swap(two)) if j < 8 else jnp.where(low16, swap(one), two)
            cols = slice(128 * j, 128 * (j + 1))
            v = tok[pl.ds(row, 16), cols].astype(F32) + v * scale * post[:, cols]
            tok[pl.ds(row, 16), cols] = v.astype(BF16)

    stores = []
    for half in (0, 1):
        for s, _, home in back:
            if s == half:
                home[0].arrived()
                home[1].arrived()
        for h in (0, 1):
            pl.loop(0, 8)(lambda i, h=h, half=half: finish(half, h, i))
            rows = pl.ds((2 * h + half) * 128, 128)
            stores.append(pltpu.make_async_copy(tok.at[rows], out_ref.at[rows], load.at[8 + len(stores)]))
            stores[-1].start()

    for c in A + B + C + E + zw + tok_z + tok_c + tok_f + across:
        c.left()
    for _, over, home in back:
        over.left()
        home[0].left()
        home[1].left()
    for c in stores:
        c.wait()


def shards(tokens, pre_gain, gate_weight, value_weight, down_weight, post_gain):
    any_, vmem = pl.BlockSpec(memory_space=pl.ANY), pl.BlockSpec(memory_space=pltpu.VMEM)
    sem = pltpu.SemaphoreType.DMA
    buf = lambda *s, t=BF16: pltpu.VMEM(s, t)
    return pl.pallas_call(
        kernel,
        out_shape=jax.ShapeDtypeStruct((TOK, D), BF16),
        in_specs=[any_, vmem, any_, any_, any_, vmem],
        out_specs=any_,
        scratch_shapes=[
            buf(TOK, D), buf(64, F), buf(64, F), buf(128, F), buf(2, Q, 128), buf(Q, 128), buf(2112, F), buf(768, D),
            buf(8, 2560, 256), buf(2048, F, t=F32), buf(2048, 768), *[buf(2, 4, 4, 256, 128)] * 3, *[buf(2, 2, 4, 4, 128, 128)] * 2,
            buf(TOK, D), buf(TOK, D), buf(TOK, D),
            sem((12,)), sem((4, 20)), sem((4, 20)), sem((4,)), sem((4,)), sem((12,)), sem((12,)), sem((62,)), sem((62,)),
        ],
        compiler_params=pltpu.CompilerParams(collective_id=0, has_side_effects=True, vmem_limit_bytes=63 * 1024 * 1024),
    )(tokens, pre_gain, gate_weight, value_weight, down_weight.T, post_gain)


def solution(mesh):
    rows = P(("rep", "fs", "tp"), None)
    in_specs = (rows, P(), P("fs", "tp"), P("fs", "tp"), P("tp", "fs"), P())
    return jax.shard_map(shards, mesh=mesh, in_specs=in_specs, out_specs=rows, check_vma=False)
```

time: 97.4 us -> 90.9 us (0.933)
  Pallas kernels: 91.4 us -> 87.5 us
  local copies, waits for them, and re-layouts: 5.74 us -> 3.16 us
    pallas_call x1, Pallas kernels: 91.4 us -> 87.5 us  [shards(): pl.pallas_call(kernel, out_shape=jax.ShapeDtypeStruct((TOK, D), BF16), in...]
    broadcast_in_dim x2 -> x0, local copies, waits for them, and re-layouts: 2.58 us -> none  [the longest x1 1.29 us: shards(): pre_gain[None]]
where the time goes in v2:
time: 90.9 us; the launch traced here: 90.7 us
  Pallas kernels  87.5 us (96%)
  local copies, waits for them, and re-layouts  3.16 us (3%)
    pallas_call x1, Pallas kernels, shards(): pl.pallas_call(kernel, out_shape=jax.ShapeDtypeStruct((TOK, D), BF16), in...  87.5 us
    unnamed x1, local copies, waits for them, and re-layouts  3.16 us

profile of v2, /device:TPU:1, one launch (start us, length us, event | category | flops | bytes accessed | tf_op | source)
XLA Modules:
  0.0 90.7 jit_solution(7872375456562196094)
XLA Ops:
  0.0 87.5 %shard_map.64 = bf16[512,2048]{1,0:T(8,128)(2,1)} custom-call(bf16[512,2048]{1,0:T(8,128)(2,1)} %tok_in.1, bf16[2048]{0:T(1024)(128)(2,1)} %pre_ref.1, bf16[64,1408]{1,0:T(8,128)(2,1)} %gate_in.1, bf16[64,1408]{1,0:T(8,128)(2,1)} %value_in.1, bf16[64,1408]{1,0:T(8,128)(2,1)} %bitcast.1, bf16[2048]{0:T(1024)(128)(2,1)} %post_ref.1), custom_call_target="tpu_custom_call" | custom-call | tf_op jit(solution)/shard_map/pallas_call | solution.py:454
  87.5 3.2 %copy.8 = bf16[512,2048]{1,0:T(8,128)(2,1)} copy(bf16[512,2048]{1,0:T(8,128)(2,1)} %shard_map.64) | data formatting | bytes 4194304

commit v3 on v2

v3 whole, which is shorter than its diff:
```python
import jax
import jax.numpy as jnp
from jax import lax
from jax.experimental import pallas as pl
from jax.experimental.pallas import tpu as pltpu
from jax.sharding import PartitionSpec as P

D, F, Q, TOK = 2048, 1408, 704, 512
SENT = 2048
EPS = 1e-06
F32, BF16 = jnp.float32, jnp.bfloat16


def remote_copy(src, dst, send_sem, recv_sem, to):
    return pltpu.make_async_remote_copy(src_ref=src, dst_ref=dst, send_sem=send_sem, recv_sem=recv_sem, device_id=to,
                                        device_id_type=pl.DeviceIdType.MESH)


TOGETHER = {0: (0, 2), 1: (0, 2), 4: (1, 2), 8: (1, 2), 2: (2, 1), 3: (2, 1), 5: (3, 2), 9: (3, 2), 6: (4, 2), 10: (4, 2),
            7: (5, 2), 11: (5, 2)}


def ring_copies(block, half, to_a, to_b, send, recv):
    c = []
    for way in (1, -1):
        c.append((block(0, 0, 0, 0), block(0, 0, way, 0), to_a[way]))
    for way, h in ((1, 0), (-1, 1)):
        c.append((half(-way, 0, 0, 0, h), half(-way, 0, way, 0, h), to_a[way]))
    for way in (1, -1):
        for oa in (0, -1, 1, 2):
            c.append((block(oa, 0, 0, 0), block(oa, 0, 0, way), to_b[way]))
    for way, h in ((1, 0), (-1, 1)):
        for oa in (0, -1, 1, 2):
            c.append((half(oa, -way, 0, 0, h), half(oa, -way, 0, way, h), to_b[way]))
    return [remote_copy(src, dst, send, recv(i), to) for i, (src, dst, to) in enumerate(c)]


def position(offset):
    return (0, 1, 3, 2)[offset % 4]


def kernel(tok_in, pre_ref, gate_in, value_in, down_in, post_ref, out_ref, tok, wg, wv, wd, dd, dz, w, d, t, acc, hid, ps,
           pr, rp, zs, zr, os_, or_, load, ag_r, zw_r, tk_r, pr_r, zr_r, or_r, sent):
    rep, fs, core = lax.axis_index("rep"), lax.axis_index("fs"), lax.axis_index("tp")
    zlo, y, x = fs // 16, (fs // 4) % 4, fs % 4
    z = rep * 2 + zlo

    def device(dz_=0, dy=0, dx=0, other=False):
        zz, yy, xx = (z + dz_ + 4) % 4, (y + dy + 4) % 4, (x + dx + 4) % 4
        return {"rep": zz // 2, "fs": (zz % 2) * 16 + yy * 4 + xx, "tp": 1 - core if other else core}

    to_x = {1: device(dx=1), -1: device(dx=-1)}
    to_y = {1: device(dy=1), -1: device(dy=-1)}
    to_z = {1: device(dz_=1), -1: device(dz_=-1)}
    partner = device(other=True)

    loads = [
        pltpu.make_async_copy(gate_in, wg, load.at[0]),
        pltpu.make_async_copy(value_in, wv, load.at[1]),
        pltpu.make_async_copy(down_in, wd.at[0:64], load.at[2]),
        pltpu.make_async_copy(down_in, wd.at[64:128], load.at[3]),
    ] + [pltpu.make_async_copy(tok_in.at[128 * c:128 * c + 128], tok.at[128 * c:128 * c + 128], load.at[4 + c]) for c in range(4)]
    for c in loads:
        c.start()

    barrier = pltpu.get_barrier_semaphore()
    for peer in (*to_x.values(), *to_y.values(), *to_z.values(), partner):
        pl.semaphore_signal(barrier, inc=1, device_id=peer, device_id_type=pl.DeviceIdType.MESH)

    lanes = lax.broadcasted_iota(jnp.int32, (64, 128), 1)
    low = lanes < 64
    swap = lambda v: pltpu.roll(v, 64, 1)

    loads[0].wait()
    loads[1].wait()
    place = (y * 4 + x) * 64
    for q in (0, 1):
        at = pl.multiple_of(place + (zlo + q) % 2 * (2048 - place), 64)
        g5, v5 = wg[:, 640:768].astype(F32), wv[:, 640:768].astype(F32)
        first = 768 * q
        w[pl.ds(at, 64), 0:640] = wg[:, first:first + 640]
        w[pl.ds(at, 64), 640:1280] = wv[:, first:first + 640]
        mixed = jnp.where(low, g5, swap(v5)) if q == 0 else jnp.where(low, swap(g5), v5)
        w[pl.ds(at, 64), 1280:1408] = mixed.astype(BF16)

    def slot(oy, ox):
        return (y + oy + 4) % 4, (x + ox + 4) % 4

    def gv(first, rows, h):
        def ref(oa, ob, ma, mb):
            yy, xx = slot(ob, oa) if first == "x" else slot(oa, ob)
            at = (yy * 4 + xx) * 64 if first == "x" else 1024 + (xx * 4 + yy) * 64
            return w.at[pl.ds(pl.multiple_of(at + h * rows, rows), rows)]

        return ref

    def dn(first, rows, h):
        def ref(oa, ob, ma, mb):
            oa, ob = position(oa - ma), position(ob - mb)
            at = (0 if first == "x" else 352) + h * rows
            n = (ob * 4 + oa if first == "x" else oa * 4 + ob) * 128
            return d.at[at:at + rows, n:n + 128]

        return ref

    def arrived(ref, sem):
        remote_copy(ref, ref, sem, sem, partner).wait_recv()

    def left(ref, sem):
        remote_copy(ref, ref, sem, sem, partner).wait_send()

    def together(i, kind):
        if i in TOGETHER:
            return TOGETHER[i]
        if kind is gv:
            return 6, 4
        return (6, 1) if i in (12, 16) else (7, 3)

    items = []
    for i, (make, rows, first) in enumerate(((gv, 64, "x"), (gv, 64, "y"), (dn, 352, "x"), (dn, 352, "y"))):
        halves = [make(first, rows // 2, h) for h in (0, 1)]
        half = lambda oa, ob, ma, mb, h, halves=halves: halves[h](oa, ob, ma, mb)
        a, b = (to_x, to_y) if first == "x" else (to_y, to_x)
        sem = lambda n, i=i, make=make: ag_r.at[i, together(n, make)[0]]
        items.append((ring_copies(make(first, rows, 0), half, a, b, sent.at[i // 2], sem), make, i))
    A, B, C, E = items

    def send(item, *which):
        for i in which:
            item[0][i].start()

    def recv(item, which):
        group, blocks = together(which, item[1])
        ref = w.at[0:64 * blocks] if item[1] is gv else d.at[0:352, 0:128 * blocks]
        arrived(ref, ag_r.at[item[2], group])

    def rows_of(ref, at, n):
        return ref.at[pl.ds(pl.multiple_of(at, n), n)]

    zw = []
    for h, way in ((0, 1), (1, -1)):
        dst = rows_of(w, 1024 + (x * 4 + y) * 64 + 32 * h, 32)
        zw.append(remote_copy(w.at[2048 + 32 * h:2080 + 32 * h], dst, sent.at[2], zw_r.at[0], to_z[way]))
    for h, way in ((0, 1), (1, -1)):
        part = pl.ds(352 * h, 352)
        zw.append(remote_copy(dd.at[1 - zlo, part], dz.at[part], sent.at[2], zw_r.at[1], to_z[way]))

    def group_rows(at):
        return t.at[:, pl.ds(at, 128)]

    tok_z, tok_c, tok_f = [], [], []
    for c in range(4):
        r = 128 * c
        mine = 1024 + 512 * (c % 2) + 128 * (c // 2)
        tok_z.append(remote_copy(group_rows(SENT + r), group_rows(mine), sent.at[3], tk_r.at[c % 2], to_z[1 if c < 2 else -1]))
        tok_c.append(remote_copy(group_rows(r), group_rows(512 + r), sent.at[3], tk_r.at[2], partner))
        tok_f.append(remote_copy(group_rows(mine), group_rows(mine + 256), sent.at[3], tk_r.at[3 + c % 2], partner))

    def forward(half):
        arrived(t.at[:, 0:256], tk_r.at[half])
        tok_f[half].start()
        tok_f[half + 2].start()

    def forwarded(half):
        arrived(t.at[:, 0:256], tk_r.at[3 + half])

    gain = pre_ref[...].astype(F32).reshape(1, D)
    low32 = lax.broadcasted_iota(jnp.int32, (32, 128), 1) < 64

    def norm_rows(r):
        v = tok[pl.ds(r, 32), :].astype(F32)
        v = v * lax.rsqrt(jnp.mean(v * v, axis=-1, keepdims=True) + EPS) * gain
        for k in (0, 1):
            straight = pl.multiple_of((zlo + k) % 2 * SENT + r, 32)
            turned = pl.multiple_of((zlo + k + 1) % 2 * SENT + r, 32)
            tiles = [v[:, k * 1024 + 128 * i:k * 1024 + 128 * (i + 1)] for i in range(8)]
            flipped = [swap(s) for s in tiles]
            for i in range(8):
                t[i // 2, pl.ds(straight, 32), 128 * (i % 2):128 * (i % 2 + 1)] = tiles[i].astype(BF16)
            for xx in range(4):
                for p in (0, 1):
                    one, two = 4 * p + xx // 2, 4 * p + 2 + xx // 2
                    if xx % 2 == 0:
                        out = jnp.where(low32, tiles[one], flipped[two])
                    else:
                        out = jnp.where(low32, flipped[one], tiles[two])
                    t[4 + xx, pl.ds(turned, 32), 128 * p:128 * (p + 1)] = out.astype(BF16)

    def norm(c):
        loads[4 + c].wait()
        pl.loop(0, 4)(lambda i: norm_rows(pl.multiple_of(c * 128 + i * 32, 32)))

    def gates(groups, row, count, first):
        def step(i):
            r = pl.multiple_of(row + i * 512, 512)
            for n in range(0, F, 256):
                m = min(256, F - n)
                total = None if first else acc[pl.ds(r, 512), n:n + m]
                for g in groups:
                    part = jnp.dot(t[g, pl.ds(r, 512), :], w[pl.ds(pl.multiple_of(g * 256, 256), 256), n:n + m],
                                   preferred_element_type=F32)
                    total = part if total is None else total + part
                acc[pl.ds(r, 512), n:n + m] = total

        pl.loop(0, count // 512)(step)

    low128 = lax.broadcasted_iota(jnp.int32, (128, 128), 1) < 64

    def hide(row, count):
        def step(i):
            r = pl.multiple_of(row + i * 128, 128)
            for n in range(0, 640, 128):
                g = acc[pl.ds(r, 128), n:n + 128]
                h = g / (1 + jnp.exp(-g)) * acc[pl.ds(r, 128), 640 + n:768 + n]
                hid[pl.ds(r, 128), n:n + 128] = h.astype(BF16)
            m = acc[pl.ds(r, 128), 1280:1408]
            h = m / (1 + jnp.exp(-m)) * swap(m)
            hid[pl.ds(r, 128), 640:768] = jnp.where(low128, h, 0).astype(BF16)

        pl.loop(0, count // 128)(step)

    one, two, last = slice(0, 1), slice(1, 3), slice(3, 4)
    steps = (((one, one),), ((one, two), (two, one)), ((two, two),), ((two, last), (last, two)),
             ((one, last), (last, one), (last, last)))

    def slots_of(parts):
        return [(py, px) for rows, cols in parts for py in range(4)[rows] for px in range(4)[cols]]

    def remote(s, n):
        slots = slots_of(steps[n])
        right = jnp.concatenate([d[:, (py * 4 + px) * 128:(py * 4 + px + 1) * 128] for py, px in slots], axis=1)
        part = jnp.dot(hid[1024 + 512 * s:1536 + 512 * s, :], right, preferred_element_type=F32).astype(BF16)
        for i, (py, px) in enumerate(slots):
            ps[s, py, px] = part[256:512, 128 * i:128 * (i + 1)]
            rp[s, py, px] = part[0:256, 128 * i:128 * (i + 1)]
        for rows, cols in steps[n]:
            remote_copy(ps.at[s, rows, cols], pr.at[s, rows, cols], sent.at[4], pr_r.at[s, n], partner).start()

    def pass_on(s, n):
        slots = slots_of(steps[n])
        arrived(pr.at[s, 0, 0:len(slots)], pr_r.at[s, n])
        for py, px in slots:
            both = (rp[s, py, px].astype(F32) + pr[s, py, px].astype(F32)).astype(BF16)
            zs[s, 0, py, px] = both[0:128]
            zs[s, 1, py, px] = both[128:256]
        for rows, cols in steps[n]:
            for h, way in ((0, -1), (1, 1)):
                remote_copy(zs.at[s, h, rows, cols], zr.at[s, h, rows, cols], sent.at[5], zr_r.at[s], to_z[way]).start()

    norm(0)
    pl.semaphore_wait(barrier, 7)
    zw[0].start()
    zw[1].start()
    send(A, 0, 1, 4, 8)
    tok_z[0].start()
    tok_c[0].start()
    for c in (2, 1, 3):
        norm(c)
        tok_z[c].start()
        tok_c[c].start()

    loads[2].wait()
    loads[3].wait()
    for i in range(11):
        turned = wd[:, i * 128:(i + 1) * 128].astype(F32).T.astype(BF16)
        at = i * 128
        if i < 5:
            dd[0, at:at + 128] = turned
        elif i == 5:
            dd[0, 640:704] = turned[0:64]
            dd[1, 640:704] = turned[64:128]
        else:
            dd[1, at - 768:at - 640] = turned
    zw[2].start()
    zw[3].start()
    d[Q:768, :] = jnp.zeros((64, D), BF16)

    arrived(w.at[0:64], zw_r.at[0])
    send(B, 0, 1, 4, 8)
    recv(A, 0)
    send(A, 2, 3, 5, 9)
    recv(B, 0)
    send(B, 2, 3, 5, 9)
    recv(A, 4)
    send(A, 6, 10, 12, 16)
    recv(B, 4)
    send(B, 6, 10, 12, 16)
    arrived(t.at[:, 0:512], tk_r.at[2])
    recv(A, 2)
    send(A, 7, 11)
    recv(A, 5)
    send(A, 13, 17)
    recv(B, 2)
    send(B, 7, 11)
    here, near, far = (y, 4 + x), ((y + 1) % 4, (y + 3) % 4, 4 + (x + 1) % 4, 4 + (x + 3) % 4), ((y + 2) % 4, 4 + (x + 2) % 4)
    gates(here, 0, 512, True)
    recv(B, 5)
    send(B, 13, 17)
    forward(0)
    gates(here, 512, 512, True)
    recv(A, 6)
    send(A, 14, 18)
    forwarded(0)
    gates(here, 1024, 512, True)
    recv(B, 6)
    send(B, 14, 18)
    recv(A, 7)
    send(A, 15, 19)
    recv(B, 7)
    send(B, 15, 19)
    gates(near, 1024, 512, False)
    forward(1)

    arrived(dz, zw_r.at[1])
    own_half = (lax.broadcasted_iota(jnp.int32, (Q, 128), 1) < 64) == (zlo == 0)
    d[0:Q, 0:128] = jnp.where(own_half, dd[zlo].astype(F32), dz[...].astype(F32)).astype(BF16)
    send(C, 0, 1)
    send(E, 0, 1)
    send(C, 4, 8)
    send(E, 4, 8)
    forwarded(1)
    gates(here + near, 1536, 512, True)
    recv(A, 12)
    recv(B, 12)
    gates(far, 1024, 512, False)
    hide(1024, 512)
    remote(0, 0)
    gates(far, 1536, 512, False)
    pass_on(0, 0)
    hide(1536, 512)
    remote(1, 0)
    recv(C, 0)
    send(C, 2, 3, 5, 9)
    recv(E, 0)
    send(E, 2, 3, 5, 9)
    recv(C, 4)
    send(C, 6, 10, 12, 16)
    recv(E, 4)
    send(E, 6, 10, 12, 16)
    remote(0, 1)
    pass_on(1, 0)
    remote(1, 1)
    pass_on(0, 1)
    recv(C, 2)
    send(C, 7, 11)
    recv(E, 2)
    send(E, 7, 11)
    pass_on(1, 1)
    recv(C, 5)
    send(C, 13, 17)
    recv(E, 5)
    send(E, 13, 17)
    gates(near, 0, 512, False)
    recv(C, 6)
    send(C, 14, 18)
    recv(E, 6)
    send(E, 14, 18)
    remote(0, 2)
    gates(near, 512, 512, False)
    pass_on(0, 2)
    remote(1, 2)
    recv(C, 7)
    send(C, 15, 19)
    recv(E, 7)
    send(E, 15, 19)
    gates(far, 0, 512, False)
    pass_on(1, 2)
    gates(far, 512, 512, False)
    hide(0, 1024)
    recv(C, 12)
    recv(E, 12)
    recv(C, 13)
    recv(E, 13)
    remote(0, 3)
    remote(0, 4)
    pass_on(0, 3)
    remote(1, 3)
    pass_on(0, 4)
    remote(1, 4)
    pass_on(1, 3)

    for n in range(4):
        cols = slice(512 * n, 512 * (n + 1))
        os_[:, cols] = jnp.dot(hid[512:1024, :], d[:, cols], preferred_element_type=F32).astype(BF16)
        remote_copy(os_.at[:, cols], or_.at[:, cols], sent.at[6], or_r.at[0], partner).start()
        place = slice(512 * (n % 2), 512 * (n % 2 + 1))
        acc[1024 + 512 * (n // 2):1536 + 512 * (n // 2), place] = jnp.dot(hid[0:512, :], d[:, cols], preferred_element_type=F32)
        if n == 0:
            pass_on(1, 4)
    arrived(or_, or_r.at[0])

    post = post_ref[...].astype(F32).reshape(1, D)
    low16 = lax.broadcasted_iota(jnp.int32, (16, 128), 1) < 64

    def spot(theirs, me):
        o = (theirs - me + 4) % 4
        return o + o // 2 - o // 3 * 2

    spots = [(spot(j // 4, y), spot(j % 4, x)) for j in range(16)]

    def finish(s, h, i):
        r = pl.multiple_of(i * 16, 16)
        row = pl.multiple_of((2 * h + s) * 128 + r, 16)
        b, square = [], jnp.zeros((16, 128), F32)
        for py, px in spots:
            cols = pl.ds(pl.multiple_of((py * 4 + px) * 128, 128), 128)
            mine = acc[pl.ds(1024 + py // 2 * 512 + row, 16), pl.ds(pl.multiple_of((py % 2 * 4 + px) * 128, 128), 128)]
            v = mine + or_[pl.ds(row, 16), cols].astype(F32)
            b.append((v + zr[s, h, py, px, pl.ds(r, 16), :].astype(F32)).astype(BF16))
            v = b[-1].astype(F32)
            square += v * v
        scale = 0.5 * lax.rsqrt(jnp.sum(square, axis=-1, keepdims=True) * (1 / D) + EPS)
        for j in range(16):
            one, two = b[2 * (j % 8)].astype(F32), b[2 * (j % 8) + 1].astype(F32)
            v = jnp.where(low16, one, swap(two)) if j < 8 else jnp.where(low16, swap(one), two)
            cols = slice(128 * j, 128 * (j + 1))
            v = tok[pl.ds(row, 16), cols].astype(F32) + v * scale * post[:, cols]
            out_ref[pl.ds(row, 16), cols] = v.astype(BF16)

    for s in (0, 1):
        arrived(zr.at[s], zr_r.at[s])
        for h in (0, 1):
            pl.loop(0, 8, unroll=2)(lambda i, s=s, h=h: finish(s, h, i))

    left(w.at[0:1920], sent.at[0])
    left(w.at[0:960], sent.at[1])
    left(w.at[0:128], sent.at[2])
    left(t.at[:, 0:1536], sent.at[3])
    left(ps, sent.at[4])
    left(zs, sent.at[5])
    left(os_, sent.at[6])


def shards(tokens, pre_gain, gate_weight, value_weight, down_weight, post_gain):
    any_, vmem = pl.BlockSpec(memory_space=pl.ANY), pl.BlockSpec(memory_space=pltpu.VMEM)
    sem = pltpu.SemaphoreType.DMA
    buf = lambda *s, t=BF16: pltpu.VMEM(s, t)
    return pl.pallas_call(
        kernel,
        out_shape=pltpu.VMEM((TOK, D), BF16),
        in_specs=[any_, vmem, any_, any_, any_, vmem],
        out_specs=vmem,
        scratch_shapes=[
            buf(TOK, D), buf(64, F), buf(64, F), buf(128, F), buf(2, Q, 128), buf(Q, 128), buf(2112, F), buf(768, D),
            buf(8, 2560, 256), buf(2048, F, t=F32), buf(2048, 768), *[buf(2, 4, 4, 256, 128)] * 3, *[buf(2, 2, 4, 4, 128, 128)] * 2,
            buf(TOK, D), buf(TOK, D),
            sem((8,)), sem((4, 8)), sem((2,)), sem((5,)), sem((2, 5)), sem((2,)), sem((1,)), sem((7,)),
        ],
        compiler_params=pltpu.CompilerParams(collective_id=0, has_side_effects=True, vmem_limit_bytes=61 * 1024 * 1024),
    )(tokens, pre_gain, gate_weight, value_weight, down_weight.T, post_gain)


def solution(mesh):
    rows = P(("rep", "fs", "tp"), None)
    in_specs = (rows, P(), P("fs", "tp"), P("fs", "tp"), P("tp", "fs"), P())
    return jax.shard_map(shards, mesh=mesh, in_specs=in_specs, out_specs=rows, check_vma=False)
```

time: 90.9 us -> 80 us (0.88)
  Pallas kernels: 87.5 us -> 78.5 us
  local copies, waits for them, and re-layouts: 3.16 us -> 1.32 us
    pallas_call x1, Pallas kernels: 87.5 us -> 78.5 us  [shards(): pl.pallas_call(kernel, out_shape=pltpu.VMEM((TOK, D), BF16), in_specs=[an...]
    unnamed x1, local copies, waits for them, and re-layouts: 3.16 us -> 1.32 us
where the time goes in v3:
time: 80 us; the launch traced here: 79.9 us
  Pallas kernels  78.5 us (98%)
  local copies, waits for them, and re-layouts  1.32 us (2%)
    pallas_call x1, Pallas kernels, shards(): pl.pallas_call(kernel, out_shape=pltpu.VMEM((TOK, D), BF16), in_specs=[an...  78.5 us

profile of v3, /device:TPU:1, one launch (start us, length us, event | category | flops | bytes accessed | tf_op | source)
XLA Modules:
  0.0 79.9 jit_solution(5440703240357554634)
XLA Ops:
  0.0 78.5 %shard_map.64 = bf16[512,2048]{1,0:T(8,128)(2,1)S(1)} custom-call(bf16[512,2048]{1,0:T(8,128)(2,1)} %tok_in.1, bf16[2048]{0:T(1024)(128)(2,1)} %pre_ref.1, bf16[64,1408]{1,0:T(8,128)(2,1)} %gate_in.1, bf16[64,1408]{1,0:T(8,128)(2,1)} %value_in.1, bf16[64,1408]{1,0:T(8,128)(2,1)} %bitcast.1, bf16[2048]{0:T(1024)(128)(2,1)} %post_ref.1), custom_call_target="tpu_custom_call" | custom-call | tf_op jit(solution)/shard_map/pallas_call | solution.py:438
  78.5 1.3 %copy.8 = bf16[512,2048]{1,0:T(8,128)(2,1)} copy(bf16[512,2048]{1,0:T(8,128)(2,1)S(1)} %shard_map.64) | data formatting | bytes 4194304

commit v4 on v3

--- a/solution.py
+++ b/solution.py
@@ -191,18 +191,14 @@
         pl.loop(0, 4)(lambda i: norm_rows(pl.multiple_of(c * 128 + i * 32, 32)))
 
     def gates(groups, row, count, first):
-        def step(i):
-            r = pl.multiple_of(row + i * 512, 512)
-            for n in range(0, F, 256):
-                m = min(256, F - n)
-                total = None if first else acc[pl.ds(r, 512), n:n + m]
-                for g in groups:
-                    part = jnp.dot(t[g, pl.ds(r, 512), :], w[pl.ds(pl.multiple_of(g * 256, 256), 256), n:n + m],
-                                   preferred_element_type=F32)
-                    total = part if total is None else total + part
-                acc[pl.ds(r, 512), n:n + m] = total
-
-        pl.loop(0, count // 512)(step)
+        for n in range(0, F, 256):
+            m = min(256, F - n)
+            total = None if first else acc[row:row + count, n:n + m]
+            for g in groups:
+                part = jnp.dot(t[g, row:row + count, :], w[pl.ds(pl.multiple_of(g * 256, 256), 256), n:n + m],
+                               preferred_element_type=F32)
+                total = part if total is None else total + part
+            acc[row:row + count, n:n + m] = total
 
     low128 = lax.broadcasted_iota(jnp.int32, (128, 128), 1) < 64
 
@@ -220,8 +216,8 @@
         pl.loop(0, count // 128)(step)
 
     one, two, last = slice(0, 1), slice(1, 3), slice(3, 4)
-    steps = (((one, one),), ((one, two), (two, one)), ((two, two),), ((two, last), (last, two)),
-             ((one, last), (last, one), (last, last)))
+    steps = (((one, one),), ((one, two), (two, one)), ((two, two),), ((one, last), (last, one)),
+             ((two, last), (last, two), (last, last)))
 
     def slots_of(parts):
         return [(py, px) for rows, cols in parts for py in range(4)[rows] for px in range(4)[cols]]
@@ -238,7 +234,7 @@
 
     def pass_on(s, n):
         slots = slots_of(steps[n])
-        arrived(pr.at[s, 0, 0:len(slots)], pr_r.at[s, n])
+        arrived(pr.at[s, :, 0] if len(slots) == 4 else d.at[0:256, 0:128 * len(slots)], pr_r.at[s, n])
         for py, px in slots:
             both = (rp[s, py, px].astype(F32) + pr[s, py, px].astype(F32)).astype(BF16)
             zs[s, 0, py, px] = both[0:128]
@@ -252,10 +248,11 @@
     zw[0].start()
     zw[1].start()
     send(A, 0, 1, 4, 8)
-    tok_z[0].start()
     tok_c[0].start()
     for c in (2, 1, 3):
         norm(c)
+        if c == 2:
+            tok_z[0].start()
         tok_z[c].start()
         tok_c[c].start()
 
@@ -308,8 +305,8 @@
     send(A, 15, 19)
     recv(B, 7)
     send(B, 15, 19)
+    forward(1)
     gates(near, 1024, 512, False)
-    forward(1)
 
     arrived(dz, zw_r.at[1])
     own_half = (lax.broadcasted_iota(jnp.int32, (Q, 128), 1) < 64) == (zlo == 0)
@@ -318,17 +315,14 @@
     send(E, 0, 1)
     send(C, 4, 8)
     send(E, 4, 8)
+    gates(here + near, 1536, 256, True)
     forwarded(1)
-    gates(here + near, 1536, 512, True)
+    gates(here + near, 1792, 256, True)
     recv(A, 12)
     recv(B, 12)
     gates(far, 1024, 512, False)
     hide(1024, 512)
     remote(0, 0)
-    gates(far, 1536, 512, False)
-    pass_on(0, 0)
-    hide(1536, 512)
-    remote(1, 0)
     recv(C, 0)
     send(C, 2, 3, 5, 9)
     recv(E, 0)
@@ -338,46 +332,51 @@
     recv(E, 4)
     send(E, 6, 10, 12, 16)
     remote(0, 1)
-    pass_on(1, 0)
+    gates(far, 1536, 512, False)
+    pass_on(0, 0)
+    pass_on(0, 1)
+    hide(1536, 512)
+    remote(1, 0)
     remote(1, 1)
-    pass_on(0, 1)
     recv(C, 2)
     send(C, 7, 11)
     recv(E, 2)
     send(E, 7, 11)
+    pass_on(1, 0)
     pass_on(1, 1)
     recv(C, 5)
     send(C, 13, 17)
     recv(E, 5)
     send(E, 13, 17)
-    gates(near, 0, 512, False)
     recv(C, 6)
     send(C, 14, 18)
     recv(E, 6)
     send(E, 14, 18)
     remote(0, 2)
-    gates(near, 512, 512, False)
+    remote(1, 2)
+    gates(near, 0, 512, False)
     pass_on(0, 2)
-    remote(1, 2)
+    pass_on(1, 2)
     recv(C, 7)
     send(C, 15, 19)
     recv(E, 7)
     send(E, 15, 19)
-    gates(far, 0, 512, False)
-    pass_on(1, 2)
-    gates(far, 512, 512, False)
-    hide(0, 1024)
     recv(C, 12)
     recv(E, 12)
+    remote(0, 3)
+    remote(1, 3)
+    gates(near, 512, 512, False)
+    pass_on(0, 3)
+    pass_on(1, 3)
+    gates(far, 0, 512, False)
     recv(C, 13)
     recv(E, 13)
-    remote(0, 3)
     remote(0, 4)
-    pass_on(0, 3)
-    remote(1, 3)
+    remote(1, 4)
+    gates(far, 512, 512, False)
     pass_on(0, 4)
-    remote(1, 4)
-    pass_on(1, 3)
+    pass_on(1, 4)
+    hide(0, 1024)
 
     for n in range(4):
         cols = slice(512 * n, 512 * (n + 1))
@@ -385,8 +384,6 @@
         remote_copy(os_.at[:, cols], or_.at[:, cols], sent.at[6], or_r.at[0], partner).start()
         place = slice(512 * (n % 2), 512 * (n % 2 + 1))
         acc[1024 + 512 * (n // 2):1536 + 512 * (n // 2), place] = jnp.dot(hid[0:512, :], d[:, cols], preferred_element_type=F32)
-        if n == 0:
-            pass_on(1, 4)
     arrived(or_, or_r.at[0])
 
     post = post_ref[...].astype(F32).reshape(1, D)

time: 80 us -> 73.8 us (0.922)
  Pallas kernels: 78.5 us -> 72.3 us
    pallas_call x1, Pallas kernels: 78.5 us -> 72.3 us  [shards(): pl.pallas_call(kernel, out_shape=pltpu.VMEM((TOK, D), BF16), in_specs=[an...]
where the time goes in v4:
time: 73.8 us; the launch traced here: 73.6 us
  Pallas kernels  72.3 us (98%)
  local copies, waits for them, and re-layouts  1.32 us (2%)
    pallas_call x1, Pallas kernels, shards(): pl.pallas_call(kernel, out_shape=pltpu.VMEM((TOK, D), BF16), in_specs=[an...  72.3 us

profile of v4, /device:TPU:1, one launch (start us, length us, event | category | flops | bytes accessed | tf_op | source)
XLA Modules:
  0.0 73.6 jit_solution(8700734292265943840)
XLA Ops:
  0.0 72.3 %shard_map.64 = bf16[512,2048]{1,0:T(8,128)(2,1)S(1)} custom-call(bf16[512,2048]{1,0:T(8,128)(2,1)} %tok_in.1, bf16[2048]{0:T(1024)(128)(2,1)} %pre_ref.1, bf16[64,1408]{1,0:T(8,128)(2,1)} %gate_in.1, bf16[64,1408]{1,0:T(8,128)(2,1)} %value_in.1, bf16[64,1408]{1,0:T(8,128)(2,1)} %bitcast.1, bf16[2048]{0:T(1024)(128)(2,1)} %post_ref.1), custom_call_target="tpu_custom_call" | custom-call | tf_op jit(solution)/shard_map/pallas_call | solution.py:435
  72.3 1.3 %copy.8 = bf16[512,2048]{1,0:T(8,128)(2,1)} copy(bf16[512,2048]{1,0:T(8,128)(2,1)S(1)} %shard_map.64) | data formatting | bytes 4194304

commit v5 on v4

--- a/solution.py
+++ b/solution.py
@@ -40,7 +40,7 @@
 
 
 def kernel(tok_in, pre_ref, gate_in, value_in, down_in, post_ref, out_ref, tok, wg, wv, wd, dd, dz, w, d, t, acc, hid, ps,
-           pr, rp, zs, zr, os_, or_, load, ag_r, zw_r, tk_r, pr_r, zr_r, or_r, sent):
+           pr, rp, zs, zr, os_, or_, squares, load, ag_r, zw_r, tk_r, pr_r, zr_r, or_r, sent):
     rep, fs, core = lax.axis_index("rep"), lax.axis_index("fs"), lax.axis_index("tp")
     zlo, y, x = fs // 16, (fs // 4) % 4, fs % 4
     z = rep * 2 + zlo
@@ -60,12 +60,12 @@
         pltpu.make_async_copy(down_in, wd.at[0:64], load.at[2]),
         pltpu.make_async_copy(down_in, wd.at[64:128], load.at[3]),
     ] + [pltpu.make_async_copy(tok_in.at[128 * c:128 * c + 128], tok.at[128 * c:128 * c + 128], load.at[4 + c]) for c in range(4)]
-    for c in loads:
-        c.start()
-
     barrier = pltpu.get_barrier_semaphore()
     for peer in (*to_x.values(), *to_y.values(), *to_z.values(), partner):
         pl.semaphore_signal(barrier, inc=1, device_id=peer, device_id_type=pl.DeviceIdType.MESH)
+
+    for c in loads:
+        c.start()
 
     lanes = lax.broadcasted_iota(jnp.int32, (64, 128), 1)
     low = lanes < 64
@@ -241,7 +241,7 @@
             zs[s, 1, py, px] = both[128:256]
         for rows, cols in steps[n]:
             for h, way in ((0, -1), (1, 1)):
-                remote_copy(zs.at[s, h, rows, cols], zr.at[s, h, rows, cols], sent.at[5], zr_r.at[s], to_z[way]).start()
+                remote_copy(zs.at[s, h, rows, cols], zr.at[s, h, rows, cols], sent.at[5], zr_r.at[s, n // 4], to_z[way]).start()
 
     norm(0)
     pl.semaphore_wait(barrier, 7)
@@ -332,8 +332,8 @@
     recv(E, 4)
     send(E, 6, 10, 12, 16)
     remote(0, 1)
+    pass_on(0, 0)
     gates(far, 1536, 512, False)
-    pass_on(0, 0)
     pass_on(0, 1)
     hide(1536, 512)
     remote(1, 0)
@@ -354,9 +354,9 @@
     send(E, 14, 18)
     remote(0, 2)
     remote(1, 2)
-    gates(near, 0, 512, False)
     pass_on(0, 2)
     pass_on(1, 2)
+    gates(near, 0, 512, False)
     recv(C, 7)
     send(C, 15, 19)
     recv(E, 7)
@@ -365,7 +365,7 @@
     recv(E, 12)
     remote(0, 3)
     remote(1, 3)
-    gates(near, 512, 512, False)
+    gates(far, 512, 512, False)
     pass_on(0, 3)
     pass_on(1, 3)
     gates(far, 0, 512, False)
@@ -373,8 +373,8 @@
     recv(E, 13)
     remote(0, 4)
     remote(1, 4)
-    gates(far, 512, 512, False)
     pass_on(0, 4)
+    gates(near, 512, 512, False)
     pass_on(1, 4)
     hide(0, 1024)
 
@@ -382,8 +382,10 @@
         cols = slice(512 * n, 512 * (n + 1))
         os_[:, cols] = jnp.dot(hid[512:1024, :], d[:, cols], preferred_element_type=F32).astype(BF16)
         remote_copy(os_.at[:, cols], or_.at[:, cols], sent.at[6], or_r.at[0], partner).start()
+    for n in range(4):
         place = slice(512 * (n % 2), 512 * (n % 2 + 1))
-        acc[1024 + 512 * (n // 2):1536 + 512 * (n // 2), place] = jnp.dot(hid[0:512, :], d[:, cols], preferred_element_type=F32)
+        part = jnp.dot(hid[0:512, :], d[:, 512 * n:512 * (n + 1)], preferred_element_type=F32)
+        acc[1024 + 512 * (n // 2):1536 + 512 * (n // 2), place] = part
     arrived(or_, or_r.at[0])
 
     post = post_ref[...].astype(F32).reshape(1, D)
@@ -395,29 +397,69 @@
 
     spots = [(spot(j // 4, y), spot(j % 4, x)) for j in range(16)]
 
+    early, late = slots_of(sum(steps[:4], ())), slots_of(steps[4])
+
+    def mine(row, py, px):
+        return acc.at[pl.ds(pl.multiple_of(1024 + py // 2 * 512 + row, 16), 16), (py % 2 * 4 + px) * 128:(py % 2 * 4 + px + 1) * 128]
+
+    def theirs(row, py, px):
+        return or_.at[pl.ds(row, 16), (py * 4 + px) * 128:(py * 4 + px + 1) * 128]
+
+    def places(s, h, i):
+        r = pl.multiple_of(i * 16, 16)
+        return r, pl.multiple_of((2 * h + s) * 128 + r, 16)
+
+    def prepare(s, h, i):
+        r, row = places(s, h, i)
+        square = jnp.zeros((16, 128), F32)
+        for py, px in early:
+            v = mine(row, py, px)[...] + theirs(row, py, px)[...].astype(F32)
+            v = (v + zr[s, h, py, px, pl.ds(r, 16), :].astype(F32)).astype(BF16)
+            theirs(row, py, px)[...] = v
+            square += v.astype(F32) * v.astype(F32)
+        for py, px in late:
+            mine(row, py, px)[...] += theirs(row, py, px)[...].astype(F32)
+        squares[pl.ds(row, 16), :] = square
+
     def finish(s, h, i):
-        r = pl.multiple_of(i * 16, 16)
-        row = pl.multiple_of((2 * h + s) * 128 + r, 16)
-        b, square = [], jnp.zeros((16, 128), F32)
+        r, row = places(s, h, i)
+        square = squares[pl.ds(row, 16), :]
+        for py, px in late:
+            v = (mine(row, py, px)[...] + zr[s, h, py, px, pl.ds(r, 16), :].astype(F32)).astype(BF16)
+            theirs(row, py, px)[...] = v
+            square += v.astype(F32) * v.astype(F32)
+        squares[pl.ds(row, 16), :] = square
+
+    def scales(s, h, i):
+        r, row = places(s, h, i)
+        mean = jnp.sum(squares[pl.ds(row, 16), :], axis=-1, keepdims=True) * (1 / D)
+        squares[pl.ds(row, 16), :] = jnp.broadcast_to(0.5 * lax.rsqrt(mean + EPS), (16, 128))
+
+    def write(s, h, i):
+        r, row = places(s, h, i)
+        scale = squares[pl.ds(row, 16), :]
+        b = []
         for py, px in spots:
-            cols = pl.ds(pl.multiple_of((py * 4 + px) * 128, 128), 128)
-            mine = acc[pl.ds(1024 + py // 2 * 512 + row, 16), pl.ds(pl.multiple_of((py % 2 * 4 + px) * 128, 128), 128)]
-            v = mine + or_[pl.ds(row, 16), cols].astype(F32)
-            b.append((v + zr[s, h, py, px, pl.ds(r, 16), :].astype(F32)).astype(BF16))
-            v = b[-1].astype(F32)
-            square += v * v
-        scale = 0.5 * lax.rsqrt(jnp.sum(square, axis=-1, keepdims=True) * (1 / D) + EPS)
+            b.append(or_[pl.ds(row, 16), pl.ds(pl.multiple_of((py * 4 + px) * 128, 128), 128)].astype(F32))
         for j in range(16):
-            one, two = b[2 * (j % 8)].astype(F32), b[2 * (j % 8) + 1].astype(F32)
+            one, two = b[2 * (j % 8)], b[2 * (j % 8) + 1]
             v = jnp.where(low16, one, swap(two)) if j < 8 else jnp.where(low16, swap(one), two)
             cols = slice(128 * j, 128 * (j + 1))
             v = tok[pl.ds(row, 16), cols].astype(F32) + v * scale * post[:, cols]
             out_ref[pl.ds(row, 16), cols] = v.astype(BF16)
 
     for s in (0, 1):
-        arrived(zr.at[s], zr_r.at[s])
+        arrived(d.at[0:176], zr_r.at[s, 0])
         for h in (0, 1):
-            pl.loop(0, 8, unroll=2)(lambda i, s=s, h=h: finish(s, h, i))
+            pl.loop(0, 8, unroll=2)(lambda i, s=s, h=h: prepare(s, h, i))
+    for s in (0, 1):
+        arrived(d.at[0:80], zr_r.at[s, 1])
+        for h in (0, 1):
+            pl.loop(0, 8, unroll=4)(lambda i, s=s, h=h: finish(s, h, i))
+        for h in (0, 1):
+            pl.loop(0, 8, unroll=8)(lambda i, s=s, h=h: scales(s, h, i))
+        for h in (0, 1):
+            pl.loop(0, 8, unroll=2)(lambda i, s=s, h=h: write(s, h, i))
 
     left(w.at[0:1920], sent.at[0])
     left(w.at[0:960], sent.at[1])
@@ -440,8 +482,8 @@
         scratch_shapes=[
             buf(TOK, D), buf(64, F), buf(64, F), buf(128, F), buf(2, Q, 128), buf(Q, 128), buf(2112, F), buf(768, D),
             buf(8, 2560, 256), buf(2048, F, t=F32), buf(2048, 768), *[buf(2, 4, 4, 256, 128)] * 3, *[buf(2, 2, 4, 4, 128, 128)] * 2,
-            buf(TOK, D), buf(TOK, D),
-            sem((8,)), sem((4, 8)), sem((2,)), sem((5,)), sem((2, 5)), sem((2,)), sem((1,)), sem((7,)),
+            buf(TOK, D), buf(TOK, D), buf(TOK, 128, t=F32),
+            sem((8,)), sem((4, 8)), sem((2,)), sem((5,)), sem((2, 5)), sem((2, 2)), sem((1,)), sem((7,)),
         ],
         compiler_params=pltpu.CompilerParams(collective_id=0, has_side_effects=True, vmem_limit_bytes=61 * 1024 * 1024),
     )(tokens, pre_gain, gate_weight, value_weight, down_weight.T, post_gain)

time: 73.8 us -> 74.4 us (level)
  no operation moved by 1% of the time
where the time goes in v5:
time: 74.4 us; the launch traced here: 74.2 us
  Pallas kernels  72.9 us (98%)
  local copies, waits for them, and re-layouts  1.32 us (2%)
    pallas_call x1, Pallas kernels, shards(): pl.pallas_call(kernel, out_shape=pltpu.VMEM((TOK, D), BF16), in_specs=[an...  72.9 us

profile of v5, /device:TPU:1, one launch (start us, length us, event | category | flops | bytes accessed | tf_op | source)
XLA Modules:
  0.0 74.2 jit_solution(16071342192186998224)
XLA Ops:
  0.0 72.9 %shard_map.64 = bf16[512,2048]{1,0:T(8,128)(2,1)S(1)} custom-call(bf16[512,2048]{1,0:T(8,128)(2,1)} %tok_in.1, bf16[2048]{0:T(1024)(128)(2,1)} %pre_ref.1, bf16[64,1408]{1,0:T(8,128)(2,1)} %gate_in.1, bf16[64,1408]{1,0:T(8,128)(2,1)} %value_in.1, bf16[64,1408]{1,0:T(8,128)(2,1)} %bitcast.1, bf16[2048]{0:T(1024)(128)(2,1)} %post_ref.1), custom_call_target="tpu_custom_call" | custom-call | tf_op jit(solution)/shard_map/pallas_call | solution.py:477
  72.9 1.3 %copy.8 = bf16[512,2048]{1,0:T(8,128)(2,1)} copy(bf16[512,2048]{1,0:T(8,128)(2,1)S(1)} %shard_map.64) | data formatting | bytes 4194304

commit v6 on v5

--- a/solution.py
+++ b/solution.py
@@ -354,9 +354,9 @@
     send(E, 14, 18)
     remote(0, 2)
     remote(1, 2)
+    gates(near, 0, 512, False)
     pass_on(0, 2)
     pass_on(1, 2)
-    gates(near, 0, 512, False)
     recv(C, 7)
     send(C, 15, 19)
     recv(E, 7)
@@ -365,17 +365,17 @@
     recv(E, 12)
     remote(0, 3)
     remote(1, 3)
-    gates(far, 512, 512, False)
+    gates(near, 512, 512, False)
     pass_on(0, 3)
     pass_on(1, 3)
-    gates(far, 0, 512, False)
     recv(C, 13)
     recv(E, 13)
     remote(0, 4)
     remote(1, 4)
+    gates(far, 0, 512, False)
     pass_on(0, 4)
-    gates(near, 512, 512, False)
     pass_on(1, 4)
+    gates(far, 512, 512, False)
     hide(0, 1024)
 
     for n in range(4):

time: 74.4 us -> 72.9 us (0.980)
  Pallas kernels: 72.9 us -> 71.4 us
    pallas_call x1, Pallas kernels: 72.9 us -> 71.4 us  [shards(): pl.pallas_call(kernel, out_shape=pltpu.VMEM((TOK, D), BF16), in_specs=[an...]
where the time goes in v6:
time: 72.9 us; the launch traced here: 72.7 us
  Pallas kernels  71.4 us (98%)
  local copies, waits for them, and re-layouts  1.32 us (2%)
    pallas_call x1, Pallas kernels, shards(): pl.pallas_call(kernel, out_shape=pltpu.VMEM((TOK, D), BF16), in_specs=[an...  71.4 us

profile of v6, /device:TPU:1, one launch (start us, length us, event | category | flops | bytes accessed | tf_op | source)
XLA Modules:
  0.0 72.7 jit_solution(7032229519337669669)
XLA Ops:
  0.0 71.4 %shard_map.64 = bf16[512,2048]{1,0:T(8,128)(2,1)S(1)} custom-call(bf16[512,2048]{1,0:T(8,128)(2,1)} %tok_in.1, bf16[2048]{0:T(1024)(128)(2,1)} %pre_ref.1, bf16[64,1408]{1,0:T(8,128)(2,1)} %gate_in.1, bf16[64,1408]{1,0:T(8,128)(2,1)} %value_in.1, bf16[64,1408]{1,0:T(8,128)(2,1)} %bitcast.1, bf16[2048]{0:T(1024)(128)(2,1)} %post_ref.1), custom_call_target="tpu_custom_call" | custom-call | tf_op jit(solution)/shard_map/pallas_call | solution.py:477
  71.4 1.3 %copy.8 = bf16[512,2048]{1,0:T(8,128)(2,1)} copy(bf16[512,2048]{1,0:T(8,128)(2,1)S(1)} %shard_map.64) | data formatting | bytes 4194304

commit v7 on v6

--- a/solution.py
+++ b/solution.py
@@ -365,7 +365,7 @@
     recv(E, 12)
     remote(0, 3)
     remote(1, 3)
-    gates(near, 512, 512, False)
+    gates(near + far, 512, 512, False)
     pass_on(0, 3)
     pass_on(1, 3)
     recv(C, 13)
@@ -375,7 +375,6 @@
     gates(far, 0, 512, False)
     pass_on(0, 4)
     pass_on(1, 4)
-    gates(far, 512, 512, False)
     hide(0, 1024)
 
     for n in range(4):
@@ -451,7 +450,7 @@
     for s in (0, 1):
         arrived(d.at[0:176], zr_r.at[s, 0])
         for h in (0, 1):
-            pl.loop(0, 8, unroll=2)(lambda i, s=s, h=h: prepare(s, h, i))
+            pl.loop(0, 8, unroll=4)(lambda i, s=s, h=h: prepare(s, h, i))
     for s in (0, 1):
         arrived(d.at[0:80], zr_r.at[s, 1])
         for h in (0, 1):
@@ -459,7 +458,7 @@
         for h in (0, 1):
             pl.loop(0, 8, unroll=8)(lambda i, s=s, h=h: scales(s, h, i))
         for h in (0, 1):
-            pl.loop(0, 8, unroll=2)(lambda i, s=s, h=h: write(s, h, i))
+            pl.loop(0, 8, unroll=4)(lambda i, s=s, h=h: write(s, h, i))
 
     left(w.at[0:1920], sent.at[0])
     left(w.at[0:960], sent.at[1])

time: 72.9 us -> 72.8 us (level)
  no operation moved by 1% of the time
where the time goes in v7:
time: 72.8 us; the launch traced here: 72.6 us
  Pallas kernels  71.3 us (98%)
  local copies, waits for them, and re-layouts  1.32 us (2%)
    pallas_call x1, Pallas kernels, shards(): pl.pallas_call(kernel, out_shape=pltpu.VMEM((TOK, D), BF16), in_specs=[an...  71.3 us

profile of v7, /device:TPU:1, one launch (start us, length us, event | category | flops | bytes accessed | tf_op | source)
XLA Modules:
  0.0 72.6 jit_solution(9218991257258656304)
XLA Ops:
  0.0 71.3 %shard_map.64 = bf16[512,2048]{1,0:T(8,128)(2,1)S(1)} custom-call(bf16[512,2048]{1,0:T(8,128)(2,1)} %tok_in.1, bf16[2048]{0:T(1024)(128)(2,1)} %pre_ref.1, bf16[64,1408]{1,0:T(8,128)(2,1)} %gate_in.1, bf16[64,1408]{1,0:T(8,128)(2,1)} %value_in.1, bf16[64,1408]{1,0:T(8,128)(2,1)} %bitcast.1, bf16[2048]{0:T(1024)(128)(2,1)} %post_ref.1), custom_call_target="tpu_custom_call" | custom-call | tf_op jit(solution)/shard_map/pallas_call | solution.py:476
  71.3 1.3 %copy.8 = bf16[512,2048]{1,0:T(8,128)(2,1)} copy(bf16[512,2048]{1,0:T(8,128)(2,1)S(1)} %shard_map.64) | data formatting | bytes 4194304

commit v8 on v7

--- a/solution.py
+++ b/solution.py
@@ -228,9 +228,10 @@
         part = jnp.dot(hid[1024 + 512 * s:1536 + 512 * s, :], right, preferred_element_type=F32).astype(BF16)
         for i, (py, px) in enumerate(slots):
             ps[s, py, px] = part[256:512, 128 * i:128 * (i + 1)]
-            rp[s, py, px] = part[0:256, 128 * i:128 * (i + 1)]
         for rows, cols in steps[n]:
             remote_copy(ps.at[s, rows, cols], pr.at[s, rows, cols], sent.at[4], pr_r.at[s, n], partner).start()
+        for i, (py, px) in enumerate(slots):
+            rp[s, py, px] = part[0:256, 128 * i:128 * (i + 1)]
 
     def pass_on(s, n):
         slots = slots_of(steps[n])
@@ -450,7 +451,7 @@
     for s in (0, 1):
         arrived(d.at[0:176], zr_r.at[s, 0])
         for h in (0, 1):
-            pl.loop(0, 8, unroll=4)(lambda i, s=s, h=h: prepare(s, h, i))
+            pl.loop(0, 8, unroll=8)(lambda i, s=s, h=h: prepare(s, h, i))
     for s in (0, 1):
         arrived(d.at[0:80], zr_r.at[s, 1])
         for h in (0, 1):
@@ -458,7 +459,7 @@
         for h in (0, 1):
             pl.loop(0, 8, unroll=8)(lambda i, s=s, h=h: scales(s, h, i))
         for h in (0, 1):
-            pl.loop(0, 8, unroll=4)(lambda i, s=s, h=h: write(s, h, i))
+            pl.loop(0, 8, unroll=8)(lambda i, s=s, h=h: write(s, h, i))
 
     left(w.at[0:1920], sent.at[0])
     left(w.at[0:960], sent.at[1])

time: 72.8 us -> 72.6 us (level)
  no operation moved by 1% of the time
where the time goes in v8:
time: 72.6 us; the launch traced here: 72.4 us
  Pallas kernels  71.1 us (98%)
  local copies, waits for them, and re-layouts  1.32 us (2%)
    pallas_call x1, Pallas kernels, shards(): pl.pallas_call(kernel, out_shape=pltpu.VMEM((TOK, D), BF16), in_specs=[an...  71.1 us

profile of v8, /device:TPU:1, one launch (start us, length us, event | category | flops | bytes accessed | tf_op | source)
XLA Modules:
  0.0 72.4 jit_solution(6485708611484881417)
XLA Ops:
  0.0 71.1 %shard_map.64 = bf16[512,2048]{1,0:T(8,128)(2,1)S(1)} custom-call(bf16[512,2048]{1,0:T(8,128)(2,1)} %tok_in.1, bf16[2048]{0:T(1024)(128)(2,1)} %pre_ref.1, bf16[64,1408]{1,0:T(8,128)(2,1)} %gate_in.1, bf16[64,1408]{1,0:T(8,128)(2,1)} %value_in.1, bf16[64,1408]{1,0:T(8,128)(2,1)} %bitcast.1, bf16[2048]{0:T(1024)(128)(2,1)} %post_ref.1), custom_call_target="tpu_custom_call" | custom-call | tf_op jit(solution)/shard_map/pallas_call | solution.py:477
  71.1 1.3 %copy.8 = bf16[512,2048]{1,0:T(8,128)(2,1)} copy(bf16[512,2048]{1,0:T(8,128)(2,1)S(1)} %shard_map.64) | data formatting | bytes 4194304
